TPU v7x, 32 devices: a whole 2x2x4 slice. The times are simulated.
32 devices in a mesh: grp: 2 (over y), tp: 4 (over z), dp: 4 (over x, core).
Axes of the slice: x: 2, y: 2, z: 4, core: 2. Of those that a mesh axis runs over, the one named last changes fastest.
Arguments:
- residual_slot_vectors: bfloat16 [128, 4, 4096], P('grp', None, 'dp'), parts along dimension 0, may hold values from -25 to 25
- active_counts: int32 [128], P(('grp', 'dp')), parts along dimension 0, may hold values from 1 to 4, 96 in all
- lookup_map: bfloat16 [2, 4096, 4096], P(None, 'dp', 'tp'), may hold values from -0.09375 to 0.09375
- address_map: bfloat16 [2, 4096, 4096], P(None, 'dp', 'tp'), may hold values from -0.09375 to 0.09375
- content_map: bfloat16 [2, 4096, 4096], P(None, 'dp', 'tp'), may hold values from -0.09375 to 0.09375
- result_valve_map: bfloat16 [2, 4096, 4096], P(None, 'dp', 'tp'), may hold values from -0.09375 to 0.09375
- fading_map_coefficients: bfloat16 [2, 4096, 64], replicated, may hold values from -0.09375 to 0.09375
- writing_intensity_map: bfloat16 [2, 4096, 64], replicated, may hold values from -0.09375 to 0.09375
- result_map: bfloat16 [2, 4096, 4096], P(None, 'tp', 'dp'), may hold values from -0.09375 to 0.09375
- fading_speed_exponent: float32 [2, 64], P(None, 'tp'), may hold values from 0 to 2.3
- fading_bias: float32 [2, 64], P(None, 'tp'), may hold values from -5 to -1
- entry_scaling: bfloat16 [2, 4096], P(None, 'dp'), may hold values from 0.099609375 to 1.8984375
- per_channel_scaling: bfloat16 [2, 64], replicated, may hold values from 0.099609375 to 1.8984375
- extra_shrink_exponent: float32 [2, 128, 4, 64], P(None, ('grp', 'dp'), None, 'tp'), parts along dimension 1, may hold values from -0.7 to 0
- memory_tensors: float32 [2, 128, 64, 4096], P(None, ('grp', 'dp'), None, 'tp'), parts along dimension 1, may hold values from -0.6 to 0.6
Outputs:
- mixed_tokens: bfloat16 [128, 4, 4096], P('grp', None, 'dp'), parts along dimension 0
- new_states: float32 [2, 128, 64, 4096], P(None, ('grp', 'dp'), None, 'tp'), parts along dimension 1
There are 2 independent parts, one for each index of `grp`. A program takes and returns all parts, laid end to end along the dimension named above; an argument that names none is the same for every part. Nothing has to cross between parts.
Inputs may be any that keep to these rules, and one draw needn't show every extreme that they name: `active_counts`: every sequence has at least one live slot, at least one sequence has 4.
All inputs are finite; a program needn't handle non-finite values. No bound on the sum of `active_counts` on one device may be relied on, other than what follows from the above.
Results may differ from a plain program's by a relative error of at most 0.018.
Values may be sent and summed in bfloat16 or wider, within the bound.
A program may use at most 128 MiB of HBM per device.

v0:
```python
import jax
import jax.numpy as jnp
from jax import lax
from jax.sharding import PartitionSpec as P

D = 4096
BLOCKS = 2


EPS = 1e-06


def shortened(array):

    def short(part):
        return part.astype(jnp.bfloat16) if part.dtype == jnp.float32 else part

    return jax.tree.map(short, array)


def unit_rows(values):
    return values * lax.rsqrt(jnp.sum(values * values, axis=-1, keepdims=True) + EPS)


def recur(query, keyvec, value, fading_multiplier, beta, live, state):
    reads = []
    for step in range(query.shape[1]):
        decayed = state * jnp.exp(fading_multiplier[:, step])[:, None, :, None]
        guess = jnp.einsum(
            "skhe,shk->she", decayed, keyvec[:, step], precision=lax.Precision.HIGHEST
        )
        fresh = beta[:, step][..., None] * (value[:, step] - guess)
        updated = decayed + jnp.einsum(
            "shk,she->skhe", keyvec[:, step], fresh, precision=lax.Precision.HIGHEST
        )
        read = jnp.einsum("skhe,shk->she", updated, query[:, step], precision=lax.Precision.HIGHEST)
        alive = live[:, step]
        state = jnp.where(alive[:, None, None, None], updated, state)
        reads.append(jnp.where(alive[:, None, None], read, 0.0))
    return (jnp.stack(reads, axis=1), state)


def body(
    residual_slot_vectors,
    active_counts,
    lookup_map,
    address_map,
    content_map,
    result_valve_map,
    fading_map_coefficients,
    writing_intensity_map,
    result_map,
    fading_speed_exponent,
    fading_bias,
    entry_scaling,
    per_channel_scaling,
    extra_shrink_exponent,
    memory_tensors,
):
    all_seqs, slots, feat = residual_slot_vectors.shape
    rows_all = all_seqs * slots
    own_seqs = active_counts.shape[0]
    own_rows = own_seqs * slots
    heads_here = fading_speed_exponent.shape[1]
    head_cols = lookup_map.shape[2]
    head_size = head_cols // heads_here
    key_size = memory_tensors.shape[2]
    row_start = lax.axis_index("dp") * feat
    head_start = lax.axis_index("tp") * heads_here
    position = lax.broadcasted_iota(jnp.int32, (own_seqs, slots), 1)
    live = position < active_counts[:, None]
    resid = residual_slot_vectors.reshape(rows_all, feat)
    fresh_states = []
    for block_coefficients in range(BLOCKS):
        widened = resid.astype(jnp.float32)
        squares = jnp.sum(widened * widened, axis=1)
        scaled = (widened * entry_scaling[block_coefficients].astype(jnp.float32)).astype(
            jnp.bfloat16
        )
        decay_rows = lax.dynamic_slice(
            fading_map_coefficients[block_coefficients], (row_start, head_start), (feat, heads_here)
        )
        beta_rows = lax.dynamic_slice(
            writing_intensity_map[block_coefficients], (row_start, head_start), (feat, heads_here)
        )
        terms = tuple(
            (
                jnp.dot(scaled, weight, preferred_element_type=jnp.float32)
                for weight in (
                    lookup_map[block_coefficients],
                    address_map[block_coefficients],
                    content_map[block_coefficients],
                    result_valve_map[block_coefficients],
                    decay_rows,
                    beta_rows,
                )
            )
        )
        summed = jax.tree.map(
            lambda part: part.astype(jnp.float32),
            lax.psum_scatter(shortened(terms), "dp", scatter_dimension=0, tiled=True),
        )
        total = lax.psum(squares, "dp")
        factor_all = lax.rsqrt(total / D + EPS)
        factor = lax.dynamic_slice_in_dim(factor_all, lax.axis_index("dp") * own_rows, own_rows, 0)[
            :, None
        ]
        proj_q, proj_k, proj_v, proj_z, fading_mapped, proj_b = [part * factor for part in summed]
        query = unit_rows(
            jax.nn.silu(proj_q).reshape(own_seqs, slots, heads_here, head_size)
        ) * head_size ** (-0.5)
        keyvec = unit_rows(jax.nn.silu(proj_k).reshape(own_seqs, slots, heads_here, head_size))
        value = jax.nn.silu(proj_v).reshape(own_seqs, slots, heads_here, head_size)
        fading_multiplier = (
            -jnp.exp(fading_speed_exponent[block_coefficients])
            * jax.nn.softplus(
                fading_mapped.reshape(own_seqs, slots, heads_here) + fading_bias[block_coefficients]
            )
            + extra_shrink_exponent[block_coefficients]
        )
        beta = jax.nn.sigmoid(proj_b.reshape(own_seqs, slots, heads_here))
        state = memory_tensors[block_coefficients].reshape(
            own_seqs, key_size, heads_here, head_size
        )
        reads, state = recur(query, keyvec, value, fading_multiplier, beta, live, state)
        fresh_states.append(state.reshape(own_seqs, key_size, head_cols))
        normed = reads * lax.rsqrt(jnp.mean(reads * reads, axis=-1, keepdims=True) + EPS)
        normed = normed * per_channel_scaling[block_coefficients].astype(jnp.float32)
        gated = (normed.reshape(own_rows, head_cols) * jax.nn.silu(proj_z)).astype(jnp.bfloat16)
        out_rows = result_map[block_coefficients]
        mixed_terms = jnp.dot(
            lax.all_gather(gated, "dp", axis=0, tiled=True),
            out_rows,
            preferred_element_type=jnp.float32,
        )
        share = lax.psum_scatter(
            mixed_terms.astype(jnp.bfloat16), "tp", scatter_dimension=0, tiled=True
        ).astype(jnp.float32)
        count = share.shape[0]
        own_part = lax.dynamic_slice_in_dim(resid, lax.axis_index("tp") * count, count, 0)
        updated_rows = (own_part.astype(jnp.float32) + share).astype(jnp.bfloat16)
        resid = lax.all_gather(updated_rows, "tp", axis=0, tiled=True)
    return (resid.reshape(all_seqs, slots, feat), jnp.stack(fresh_states))


def solution(mesh):
    in_specs = (
        P("grp", None, "dp"),
        P(("grp", "dp")),
        P(None, "dp", "tp"),
        P(None, "dp", "tp"),
        P(None, "dp", "tp"),
        P(None, "dp", "tp"),
        P(),
        P(),
        P(None, "tp", "dp"),
        P(None, "tp"),
        P(None, "tp"),
        P(None, "dp"),
        P(),
        P(None, ("grp", "dp"), None, "tp"),
        P(None, ("grp", "dp"), None, "tp"),
    )
    out_specs = (P("grp", None, "dp"), P(None, ("grp", "dp"), None, "tp"))
    return jax.shard_map(body, mesh=mesh, in_specs=in_specs, out_specs=out_specs, check_vma=False)
```

profile of v0, /device:TPU:0, one launch (start us, length us, event | category | flops | bytes accessed | tf_op | source)
XLA Modules:
  0.0 578.9 jit_solution(13411621285081115818)
XLA Ops:
  7.2 1.4 slice_convert_fusion
  8.6 1.5 fusion.93
  10.2 2.1 fusion.142
  13.4 2.1 fusion.141
  16.5 3.1 fusion.68
  19.7 3.1 fusion.65
  22.9 3.1 fusion.62
  26.1 3.1 fusion.71
  32.3 8.8 %psum.14 = f32[256]{0:T(256)S(1)} all-reduce(f32[256]{0:T(256)S(1)} %reduce_sum.75), channel_id=1, replica_groups=mesh['grp'=2,'tp'=4,'dp'=4] {'dp'}, use_global_device_ids=true, to_apply=%region_2.0 | all-reduce | flops 256 | bytes 2048 | tf_op jit(solution)/shard_map/psum | solution.py:103
  41.1 8.4 %fusion.140 = (f32[1,16,64,1024]{3,2,1,0:T(8,128)}, f32[1,16,64,1024]{3,2,1,0:T(8,128)}) fusion(f32[2,16,64,1024]{3,2,1,0:T(8,128)} %param.29), kind=kLoop, calls=%fused_computation.228 | loop fusion | bytes 16777216 | tf_op jit(solution)/shard_map/slice | solution.py:122
  49.5 7.3 %reshape_squeeze.6 = f32[16,64,16,64]{3,2,1,0:T(8,128)} reshape(f32[1,16,64,1024]{3,2,1,0:T(8,128)} %get-tuple-element.17) | data formatting | bytes 8388608 | tf_op jit(solution)/shard_map/reshape;squeeze | solution.py:122
  59.5 7.5 %broadcast_multiply_fusion.7 = f32[16,64,16,64]{3,2,1,0:T(8,128)} fusion(f32[16,64,16,64]{3,2,1,0:T(8,128)} %reshape_squeeze.6, f32[16,16]{1,0:T(8,128)S(1)} %bitcast.428), kind=kLoop, calls=%fused_computation.48 | loop fusion | flops 1048576 | bytes 8389632 | tf_op jit(solution)/shard_map/mul | solution.py:28
  67.0 14.9 %reduce-scatter.27.cloned.1.call-done = bf16[64,1024]{1,0:T(8,128)(2,1)} async-done(((bf16[256,1024]{1,0:T(8,128)(2,1)}), bf16[64,1024]{1,0:T(8,128)(2,1)}) %reduce-scatter.27.cloned.1.call-update) | async-done | bytes 131088 | tf_op jit(solution)/shard_map/reduce_scatter | solution.py:101
  82.0 24.0 %reduce-scatter.25.cloned.1.call-done = bf16[64,1024]{1,0:T(8,128)(2,1)} async-done(((bf16[256,1024]{1,0:T(8,128)(2,1)}), bf16[64,1024]{1,0:T(8,128)(2,1)}) %reduce-scatter.25.cloned.1.call-update) | async-done | bytes 131088 | tf_op jit(solution)/shard_map/reduce_scatter | solution.py:101
  106.0 24.0 %reduce-scatter.23.cloned.1.call-done = bf16[64,1024]{1,0:T(8,128)(2,1)} async-done(((bf16[256,1024]{1,0:T(8,128)(2,1)}), bf16[64,1024]{1,0:T(8,128)(2,1)}) %reduce-scatter.23.cloned.1.call-update) | async-done | bytes 131088 | tf_op jit(solution)/shard_map/reduce_scatter | solution.py:101
  130.0 1.3 divide_multiply_fusion.5
  136.8 12.6 %fusion.30 = f32[16,16,1,64]{3,2,1,0:T(1,128)S(1)} fusion(f32[16,16,64,1]{2,3,1,0:T(1,128)S(1)} %bitcast.396, f32[16,64,16,64]{3,2,1,0:T(8,128)} %broadcast_multiply_fusion.7), kind=kOutput, calls=%fused_computation.39 | convolution fusion | flops 12582912 | bytes 4325376 | tf_op jit(solution)/shard_map/skhe,shk->she/dot_general | solution.py:29
  149.6 6.9 %broadcast_multiply_fusion.6 = f32[16,64,16,64]{3,2,1,0:T(8,128)S(1)} fusion(f32[16,16]{1,0:T(8,128)S(1)} %bitcast.442, f32[16,64,16,64]{3,2,1,0:T(8,128)} %reshape_squeeze.6, f32[16,16,64]{1,2,0:T(8,128)S(1)} %copy.114, f32[16,16,64]{2,1,0:T(8,128)S(1)} %fusion.119, f32[16,16]{1,0:T(8,128)S(1)} %bitcast.429, pred[16]{0:T(512)(128)(4,1)S(1)} %get-tuple-element.80), kind=kLoop, calls=%fused_computation.47 | loop fusion | flops 5242880 | bytes 8521744 | tf_op jit(solution)/shard_map/mul | solution.py:28
  156.5 9.3 %fusion.26 = f32[16,16,1,64]{3,2,1,0:T(1,128)S(1)} fusion(f32[16,16,64,1]{2,3,1,0:T(1,128)S(1)} %bitcast.394, f32[16,64,16,64]{3,2,1,0:T(8,128)S(1)} %broadcast_multiply_fusion.6), kind=kOutput, calls=%fused_computation.35 | convolution fusion | flops 12582912 | bytes 4325376 | tf_op jit(solution)/shard_map/skhe,shk->she/dot_general | solution.py:29
  166.6 6.9 %broadcast_multiply_fusion.5 = (f32[16,64,16,64]{3,2,1,0:T(8,128)S(1)}, f32[16,64,16,64]{3,2,1,0:T(8,128)S(1)}, f32[16,64,16,64]{3,2,1,0:T(8,128)S(1)}, f32[16,64,16,64]{3,2,1,0:T(8,128)S(1)}) fusion(f32[16,16]{1,0:T(8,128)S(1)} %bitcast.422, f32[16,16,64]{1,2,0:T(8,128)} %copy.117, f32[16,16,64]{2,1,0:T(8,128)} %fusion.117, f32[16,16]{1,0:T(8,128)S(1)} %bitcast.443, ...), kind=kLoop, calls=%fused_computation.46 | loop fusion | flops 9437184 | bytes 21236768 | tf_op jit(solution)/shard_map/mul | solution.py:28
  173.5 10.3 %fusion.28 = f32[16,16,1,64]{3,2,1,0:T(1,128)S(1)} fusion(f32[16,16,64,1]{2,3,1,0:T(1,128)} %bitcast.420, f32[16,64,16,64]{3,2,1,0:T(8,128)S(1)} %get-tuple-element.15), kind=kOutput, calls=%fused_computation.37 | convolution fusion | flops 12582912 | bytes 4325376 | tf_op jit(solution)/shard_map/skhe,shk->she/dot_general | solution.py:36
  183.9 9.7 %fusion.22 = f32[16,16,1,64]{3,2,1,0:T(1,128)S(1)} fusion(f32[16,16,64,1]{2,3,1,0:T(1,128)S(1)} %bitcast.392, f32[16,64,16,64]{3,2,1,0:T(8,128)S(1)} %get-tuple-element.4), kind=kOutput, calls=%fused_computation.31 | convolution fusion | flops 12582912 | bytes 4325376 | tf_op jit(solution)/shard_map/skhe,shk->she/dot_general | solution.py:29
  193.8 9.5 %fusion.24 = f32[16,16,1,64]{3,2,1,0:T(1,128)S(1)} fusion(f32[16,16,64,1]{2,3,1,0:T(1,128)S(1)} %bitcast.418, f32[16,64,16,64]{3,2,1,0:T(8,128)S(1)} %get-tuple-element.11), kind=kOutput, calls=%fused_computation.33 | convolution fusion | flops 12582912 | bytes 4325376 | tf_op jit(solution)/shard_map/skhe,shk->she/dot_general | solution.py:36
  203.2 2.9 broadcast_multiply_fusion.4
  206.2 9.3 %fusion.18 = f32[16,16,1,64]{3,2,1,0:T(1,128)S(1)} fusion(f32[16,16,64,1]{2,3,1,0:T(1,128)S(1)} %bitcast.390, f32[16,64,16,64]{3,2,1,0:T(8,128)S(1)} %broadcast_multiply_fusion.4), kind=kOutput, calls=%fused_computation.27 | convolution fusion | flops 12582912 | bytes 4325376 | tf_op jit(solution)/shard_map/skhe,shk->she/dot_general | solution.py:29
  215.6 7.4 %broadcast_select_fusion.1 = (f32[16,64,16,64]{3,2,1,0:T(8,128)}, f32[16,64,16,64]{3,2,1,0:T(8,128)S(1)}, f32[16,64,16,64]{3,2,1,0:T(8,128)S(1)}) fusion(pred[16]{0:T(512)(128)(4,1)S(1)} %copy-done.26, f32[16,64,16,64]{3,2,1,0:T(8,128)S(1)} %get-tuple-element.5, f32[16,16,64]{1,2,0:T(8,128)S(1)} %copy.118, f32[16,16,64]{2,1,0:T(8,128)S(1)} %fusion.115, ...), kind=kLoop, calls=%fused_computation.50 | loop fusion | flops 8388608 | bytes 17041440 | tf_op jit(solution)/shard_map/jit(_where)/select_n | solution.py:38
  223.1 9.3 %fusion.20 = f32[16,16,1,64]{3,2,1,0:T(1,128)S(1)} fusion(f32[16,16,64,1]{2,3,1,0:T(1,128)S(1)} %bitcast.415, f32[16,64,16,64]{3,2,1,0:T(8,128)S(1)} %get-tuple-element.12), kind=kOutput, calls=%fused_computation.29 | convolution fusion | flops 12582912 | bytes 4325376 | tf_op jit(solution)/shard_map/skhe,shk->she/dot_general | solution.py:36
  232.4 9.5 %fusion.16 = f32[16,16,1,64]{3,2,1,0:T(1,128)S(1)} fusion(f32[16,16,64,1]{2,3,1,0:T(1,128)S(1)} %bitcast.414, f32[16,64,16,64]{3,2,1,0:T(8,128)S(1)} %get-tuple-element.7), kind=kOutput, calls=%fused_computation.25 | convolution fusion | flops 12582912 | bytes 4325376 | tf_op jit(solution)/shard_map/skhe,shk->she/dot_general | solution.py:36
  242.9 1.1 multiply_convert_fusion.1
  243.9 6.5 %all_gather.12 = bf16[256,1024]{1,0:T(8,128)(2,1)S(1)} all-gather(bf16[64,1024]{1,0:T(8,128)(2,1)S(1)} %multiply_convert_fusion.1), channel_id=1, replica_groups=mesh['grp'=2,'tp'=4,'dp'=4] {'dp'}, dimensions={0}, use_global_device_ids=true | all-gather | bytes 655360 | tf_op jit(solution)/shard_map/all_gather | solution.py:132
  250.4 3.1 fusion.74
  253.8 22.4 %reduce-scatter.31.cloned.1.call-done = bf16[64,1024]{1,0:T(8,128)(2,1)} async-done(((bf16[256,1024]{1,0:T(8,128)(2,1)}), bf16[64,1024]{1,0:T(8,128)(2,1)}) %reduce-scatter.31.cloned.1.call-update) | async-done | bytes 131088 | tf_op jit(solution)/shard_map/reduce_scatter | solution.py:136
  277.2 15.5 %all_gather.13 = bf16[256,1024]{1,0:T(8,128)(2,1)S(1)} all-gather(bf16[64,1024]{1,0:T(8,128)(2,1)S(1)} %add_convert_fusion.1), channel_id=1, replica_groups=mesh['grp'=2,'tp'=4,'dp'=4] {'tp'}, dimensions={0}, use_global_device_ids=true | all-gather | bytes 655360 | tf_op jit(solution)/shard_map/all_gather | solution.py:142
  296.3 3.1 fusion.77
  299.5 3.1 fusion.80
  302.7 3.1 fusion.83
  306.6 7.3 %reshape_squeeze.7 = f32[16,64,16,64]{3,2,1,0:T(8,128)} reshape(f32[1,16,64,1024]{3,2,1,0:T(8,128)} %get-tuple-element.16) | data formatting | bytes 8388608 | tf_op jit(solution)/shard_map/reshape;squeeze | solution.py:122
  314.1 5.9 %psum.15 = f32[256]{0:T(256)S(1)} all-reduce(f32[256]{0:T(256)S(1)} %fusion.95), channel_id=1, replica_groups=mesh['grp'=2,'tp'=4,'dp'=4] {'dp'}, use_global_device_ids=true, to_apply=%region_14.15 | all-reduce | flops 256 | bytes 2048 | tf_op jit(solution)/shard_map/psum | solution.py:103
  320.1 3.1 fusion.86
  324.1 10.4 %reduce-scatter.49.cloned.1.call-done = bf16[64,16]{1,0:T(8,128)(2,1)} async-done(((bf16[256,16]{1,0:T(8,128)(2,1)}), bf16[64,16]{1,0:T(8,128)(2,1)}) %reduce-scatter.49.cloned.1.call-update) | async-done | bytes 2064
  336.2 7.5 %broadcast_multiply_fusion.3 = f32[16,64,16,64]{3,2,1,0:T(8,128)} fusion(f32[16,64,16,64]{3,2,1,0:T(8,128)} %reshape_squeeze.7, f32[16,16]{1,0:T(8,128)S(1)} %bitcast.431), kind=kLoop, calls=%fused_computation.44 | loop fusion | flops 1048576 | bytes 8389632 | tf_op jit(solution)/shard_map/mul | solution.py:28
  343.7 14.8 %reduce-scatter.33.cloned.1.call-done = bf16[64,1024]{1,0:T(8,128)(2,1)} async-done(((bf16[256,1024]{1,0:T(8,128)(2,1)}), bf16[64,1024]{1,0:T(8,128)(2,1)}) %reduce-scatter.33.cloned.1.call-update) | async-done | bytes 131088 | tf_op jit(solution)/shard_map/reduce_scatter | solution.py:101
  358.5 24.2 %reduce-scatter.35.cloned.1.call-done = bf16[64,1024]{1,0:T(8,128)(2,1)} async-done(((bf16[256,1024]{1,0:T(8,128)(2,1)}), bf16[64,1024]{1,0:T(8,128)(2,1)}) %reduce-scatter.35.cloned.1.call-update) | async-done | bytes 131088 | tf_op jit(solution)/shard_map/reduce_scatter | solution.py:101
  382.7 24.0 %reduce-scatter.37.cloned.1.call-done = bf16[64,1024]{1,0:T(8,128)(2,1)} async-done(((bf16[256,1024]{1,0:T(8,128)(2,1)}), bf16[64,1024]{1,0:T(8,128)(2,1)}) %reduce-scatter.37.cloned.1.call-update) | async-done | bytes 131088 | tf_op jit(solution)/shard_map/reduce_scatter | solution.py:101
  406.7 1.3 divide_multiply_fusion.2
  413.5 12.6 %fusion.14 = f32[16,16,1,64]{3,2,1,0:T(1,128)S(1)} fusion(f32[16,16,64,1]{2,3,1,0:T(1,128)S(1)} %bitcast.397, f32[16,64,16,64]{3,2,1,0:T(8,128)} %broadcast_multiply_fusion.3), kind=kOutput, calls=%fused_computation.23 | convolution fusion | flops 12582912 | bytes 4325376 | tf_op jit(solution)/shard_map/skhe,shk->she/dot_general | solution.py:29
  426.3 7.1 %broadcast_multiply_fusion.2 = f32[16,64,16,64]{3,2,1,0:T(8,128)S(1)} fusion(f32[16,16]{1,0:T(8,128)S(1)} %bitcast.444, f32[16,64,16,64]{3,2,1,0:T(8,128)} %reshape_squeeze.7, f32[16,16,64]{1,2,0:T(8,128)S(1)} %copy.125, f32[16,16,64]{2,1,0:T(8,128)S(1)} %fusion.111, f32[16,16]{1,0:T(8,128)S(1)} %bitcast.432, pred[16]{0:T(512)(128)(4,1)S(1)} %copy-done.23), kind=kLoop, calls=%fused_computation.43 | loop fusion | flops 5242880 | bytes 8521744 | tf_op jit(solution)/shard_map/mul | solution.py:28
  433.4 9.3 %fusion.10 = f32[16,16,1,64]{3,2,1,0:T(1,128)S(1)} fusion(f32[16,16,64,1]{2,3,1,0:T(1,128)S(1)} %bitcast.395, f32[16,64,16,64]{3,2,1,0:T(8,128)S(1)} %broadcast_multiply_fusion.2), kind=kOutput, calls=%fused_computation.19 | convolution fusion | flops 12582912 | bytes 4325376 | tf_op jit(solution)/shard_map/skhe,shk->she/dot_general | solution.py:29
  443.5 6.8 %broadcast_multiply_fusion.1 = (f32[16,64,16,64]{3,2,1,0:T(8,128)S(1)}, f32[16,64,16,64]{3,2,1,0:T(8,128)S(1)}, f32[16,64,16,64]{3,2,1,0:T(8,128)S(1)}, f32[16,64,16,64]{3,2,1,0:T(8,128)S(1)}) fusion(f32[16,16]{1,0:T(8,128)S(1)} %bitcast.425, f32[16,16,64]{1,2,0:T(8,128)} %copy.128, f32[16,16,64]{2,1,0:T(8,128)} %fusion.109, f32[16,16]{1,0:T(8,128)S(1)} %bitcast.445, ...), kind=kLoop, calls=%fused_computation.42 | loop fusion | flops 9437184 | bytes 21236768 | tf_op jit(solution)/shard_map/mul | solution.py:28
  450.4 10.3 %fusion.12 = f32[16,16,1,64]{3,2,1,0:T(1,128)S(1)} fusion(f32[16,16,64,1]{2,3,1,0:T(1,128)} %bitcast.421, f32[16,64,16,64]{3,2,1,0:T(8,128)S(1)} %get-tuple-element.14), kind=kOutput, calls=%fused_computation.21 | convolution fusion | flops 12582912 | bytes 4325376 | tf_op jit(solution)/shard_map/skhe,shk->she/dot_general | solution.py:36
  460.6 9.7 %fusion.6 = f32[16,16,1,64]{3,2,1,0:T(1,128)S(1)} fusion(f32[16,16,64,1]{2,3,1,0:T(1,128)S(1)} %bitcast.393, f32[16,64,16,64]{3,2,1,0:T(8,128)S(1)} %get-tuple-element.2), kind=kOutput, calls=%fused_computation.15 | convolution fusion | flops 12582912 | bytes 4325376 | tf_op jit(solution)/shard_map/skhe,shk->she/dot_general | solution.py:29
  470.4 9.5 %fusion.8 = f32[16,16,1,64]{3,2,1,0:T(1,128)S(1)} fusion(f32[16,16,64,1]{2,3,1,0:T(1,128)S(1)} %bitcast.419, f32[16,64,16,64]{3,2,1,0:T(8,128)S(1)} %get-tuple-element.10), kind=kOutput, calls=%fused_computation.17 | convolution fusion | flops 12582912 | bytes 4325376 | tf_op jit(solution)/shard_map/skhe,shk->she/dot_general | solution.py:36
  479.9 2.9 broadcast_multiply_fusion
  482.8 9.3 %fusion.2 = f32[16,16,1,64]{3,2,1,0:T(1,128)S(1)} fusion(f32[16,16,64,1]{2,3,1,0:T(1,128)S(1)} %bitcast.391, f32[16,64,16,64]{3,2,1,0:T(8,128)S(1)} %broadcast_multiply_fusion), kind=kOutput, calls=%fused_computation.11 | convolution fusion | flops 12582912 | bytes 4325376 | tf_op jit(solution)/shard_map/skhe,shk->she/dot_general | solution.py:29
  492.3 7.6 %broadcast_select_fusion = (f32[16,64,16,64]{3,2,1,0:T(8,128)}, f32[16,64,16,64]{3,2,1,0:T(8,128)S(1)}, f32[16,64,16,64]{3,2,1,0:T(8,128)S(1)}) fusion(pred[16]{0:T(512)(128)(4,1)S(1)} %copy-done.27, f32[16,64,16,64]{3,2,1,0:T(8,128)S(1)} %get-tuple-element.3, f32[16,16,64]{1,2,0:T(8,128)S(1)} %copy.129, f32[16,16,64]{2,1,0:T(8,128)S(1)} %fusion.107, ...), kind=kLoop, calls=%fused_computation.49 | loop fusion | flops 8388608 | bytes 17041440 | tf_op jit(solution)/shard_map/jit(_where)/select_n | solution.py:38
  499.9 9.3 %fusion.4 = f32[16,16,1,64]{3,2,1,0:T(1,128)S(1)} fusion(f32[16,16,64,1]{2,3,1,0:T(1,128)S(1)} %bitcast.417, f32[16,64,16,64]{3,2,1,0:T(8,128)S(1)} %get-tuple-element.13), kind=kOutput, calls=%fused_computation.13 | convolution fusion | flops 12582912 | bytes 4325376 | tf_op jit(solution)/shard_map/skhe,shk->she/dot_general | solution.py:36
  509.2 9.5 %fusion = f32[16,16,1,64]{3,2,1,0:T(1,128)S(1)} fusion(f32[16,16,64,1]{2,3,1,0:T(1,128)S(1)} %bitcast.416, f32[16,64,16,64]{3,2,1,0:T(8,128)S(1)} %get-tuple-element.9), kind=kOutput, calls=%fused_computation.9 | convolution fusion | flops 12582912 | bytes 4325376 | tf_op jit(solution)/shard_map/skhe,shk->she/dot_general | solution.py:36
  519.6 1.1 multiply_convert_fusion
  520.6 6.5 %all_gather.14 = bf16[256,1024]{1,0:T(8,128)(2,1)S(1)} all-gather(bf16[64,1024]{1,0:T(8,128)(2,1)S(1)} %multiply_convert_fusion), channel_id=1, replica_groups=mesh['grp'=2,'tp'=4,'dp'=4] {'dp'}, dimensions={0}, use_global_device_ids=true | all-gather | bytes 655360 | tf_op jit(solution)/shard_map/all_gather | solution.py:132
  527.2 3.1 fusion.89
  530.3 7.6 %stack_reshape.6 = f32[1,16,64,1024]{3,2,1,0:T(8,128)} reshape(f32[16,64,16,64]{3,2,1,0:T(8,128)} %get-tuple-element.6) | data formatting | bytes 8388608 | tf_op jit(solution)/shard_map/stack;reshape | solution.py:143
  537.9 7.6 %stack_reshape.7 = f32[1,16,64,1024]{3,2,1,0:T(8,128)} reshape(f32[16,64,16,64]{3,2,1,0:T(8,128)} %get-tuple-element.8) | data formatting | bytes 8388608 | tf_op jit(solution)/shard_map/stack;reshape | solution.py:143
  545.6 8.6 %pad_maximum_fusion = f32[2,16,64,1024]{3,2,1,0:T(8,128)} fusion(f32[1,16,64,1024]{3,2,1,0:T(8,128)} %stack_reshape.7, f32[1,16,64,1024]{3,2,1,0:T(8,128)} %stack_reshape.6), kind=kLoop, calls=%fused_computation | loop fusion | flops 2097152 | bytes 16777216 | tf_op jit(solution)/shard_map/stack | solution.py:143
  555.1 16.1 %all_gather.15 = bf16[256,1024]{1,0:T(8,128)(2,1)S(1)} all-gather(bf16[64,1024]{1,0:T(8,128)(2,1)S(1)} %add_convert_fusion), channel_id=1, replica_groups=mesh['grp'=2,'tp'=4,'dp'=4] {'tp'}, dimensions={0}, use_global_device_ids=true | all-gather | bytes 655360 | tf_op jit(solution)/shard_map/all_gather | solution.py:142
  (230 shorter events, 33.6 us)
Async XLA Ops:
  7.2 49.7 %reduce-scatter.43.cloned.1.call-start = ((), (), s32[]{:S(2)}) async-start(), calls=%async_computation.24 | async-start | bytes 81920
  13.3 44.5 %reduce-scatter.45.cloned.1.call-start = ((), (), s32[]{:S(2)}) async-start(), calls=%async_computation.25 | async-start | bytes 81920
  16.5 65.5 %reduce-scatter.27.cloned.1.call-start = ((), (), s32[]{:S(2)}) async-start(), calls=%async_computation.16 | async-start | bytes 655360 | tf_op jit(solution)/shard_map/reduce_scatter | solution.py:101
  19.6 9.6 %copy-start.41 = (s32[16]{0:T(128)S(1)}, s32[16]{0:T(128)}, u32[]{:S(2)}) copy-start(s32[16]{0:T(128)} %param.16) | copy-start | bytes 196
  19.6 9.7 %copy-start.39 = (f32[2,16]{1,0:T(2,128)S(1)}, f32[2,16]{1,0:T(2,128)}, u32[]{:S(2)}) copy-start(f32[2,16]{1,0:T(2,128)} %param.24) | copy-start | bytes 388
  19.6 10.2 %copy-start.40 = (f32[2,16]{1,0:T(2,128)S(1)}, f32[2,16]{1,0:T(2,128)}, u32[]{:S(2)}) copy-start(f32[2,16]{1,0:T(2,128)} %param.25) | copy-start | bytes 388
  19.6 10.8 %copy-start.37 = (bf16[2,64]{1,0:T(2,128)(2,1)S(1)}, bf16[2,64]{1,0:T(2,128)(2,1)}, u32[]{:S(2)}) copy-start(bf16[2,64]{1,0:T(2,128)(2,1)} %param.27) | copy-start | bytes 772
  19.7 86.4 %reduce-scatter.25.cloned.1.call-start = ((), (), s32[]{:S(2)}) async-start(), calls=%async_computation.15 | async-start | bytes 655360 | tf_op jit(solution)/shard_map/reduce_scatter | solution.py:101
  22.8 107.2 %reduce-scatter.23.cloned.1.call-start = ((), (), s32[]{:S(2)}) async-start(), calls=%async_computation.14 | async-start | bytes 655360 | tf_op jit(solution)/shard_map/reduce_scatter | solution.py:101
  26.0 216.8 %reduce-scatter.29.cloned.1.call-start = ((), (), s32[]{:S(2)}) async-start(), calls=%async_computation.17 | async-start | bytes 655360 | tf_op jit(solution)/shard_map/reduce_scatter | solution.py:101
  29.2 247.0 %reduce-scatter.31.cloned.1.call-start = ((), (), s32[]{:S(2)}) async-start(), calls=%async_computation.18 | async-start | bytes 655360 | tf_op jit(solution)/shard_map/reduce_scatter | solution.py:136
  31.5 118.1 %copy-start.21 = (pred[16]{0:T(512)(128)(4,1)}, pred[16]{0:T(512)(128)(4,1)S(1)}, u32[]{:S(2)}) copy-start(pred[16]{0:T(512)(128)(4,1)S(1)} %get-tuple-element.80) | copy-start | bytes 52
  49.5 9.9 %copy-start.18 = (f32[2,16,4,16]{3,2,1,0:T(4,128)S(1)}, f32[2,16,4,16]{3,2,1,0:T(4,128)}, u32[]{:S(2)}) copy-start(f32[2,16,4,16]{3,2,1,0:T(4,128)} %param.28) | copy-start | bytes 24580
  56.9 73.2 %copy-start.32 = (f32[64]{0:T(128)}, f32[64]{0:T(128)S(1)}, u32[]{:S(2)}) copy-start(f32[64]{0:T(128)S(1)} %dynamic_slice.35) | copy-start | bytes 772
  131.5 34.3 %copy-start.3 = (f32[16,4,16,64]{3,2,1,0:T(8,128)}, f32[16,4,16,64]{3,2,1,0:T(8,128)S(1)}, u32[]{:S(2)}) copy-start(f32[16,4,16,64]{3,2,1,0:T(8,128)S(1)} %reshape.241) | copy-start | bytes 786436
  149.6 17.0 %slice-start.2 = ((s8[8388608]{0:T(1024)(128)(4,1)}), s8[4194304]{0:T(1024)(128)(4,1)S(1)}, s32[]{:S(2)}) async-start(s8[8388608]{0:T(1024)(128)(4,1)} %bitcast.388), calls=%async_computation.30 | async-start | bytes 8388608
  149.6 17.0 %slice-start.3 = ((s8[8388608]{0:T(1024)(128)(4,1)}), s8[4194304]{0:T(1024)(128)(4,1)S(1)}, s32[]{:S(2)}) async-start(s8[8388608]{0:T(1024)(128)(4,1)} %bitcast.388), calls=%async_computation.31 | async-start | bytes 8388608
  173.5 10.3 %copy-start.22 = (pred[16]{0:T(512)(128)(4,1)S(1)}, pred[16]{0:T(512)(128)(4,1)}, u32[]{:S(2)}) copy-start(pred[16]{0:T(512)(128)(4,1)} %copy-done.21) | copy-start | bytes 52
  173.5 10.4 %copy-start.10 = (f32[16,1,16,64]{3,2,1,0:T(8,128)S(1)}, f32[16,1,16,64]{3,2,1,0:T(8,128)}, u32[]{:S(2)}) copy-start(f32[16,1,16,64]{3,2,1,0:T(8,128)} %get-tuple-element.38) | copy-start | bytes 196612
  173.5 20.1 %copy-start.4 = (f32[16,4,16,64]{3,2,1,0:T(8,128)S(1)}, f32[16,4,16,64]{3,2,1,0:T(8,128)}, u32[]{:S(2)}) copy-start(f32[16,4,16,64]{3,2,1,0:T(8,128)} %copy-done.3) | copy-start | bytes 786436
  173.5 20.1 %copy-start.19 = (f32[16,1,16]{2,1,0:T(1,128)S(1)}, f32[16,1,16]{2,1,0:T(1,128)}, u32[]{:S(2)}) copy-start(f32[16,1,16]{2,1,0:T(1,128)} %get-tuple-element.57) | copy-start | bytes 3076
  173.5 20.2 %copy-start.16 = (f32[16,1,16,64]{3,2,1,0:T(8,128)S(1)}, f32[16,1,16,64]{3,2,1,0:T(8,128)}, u32[]{:S(2)}) copy-start(f32[16,1,16,64]{3,2,1,0:T(8,128)} %get-tuple-element.37) | copy-start | bytes 196612
  203.2 2.9 copy-start.8
  206.2 9.4 %copy-start.1 = (f32[16,16,64]{1,2,0:T(8,128)S(1)}, f32[16,16,64]{1,2,0:T(8,128)}, u32[]{:S(2)}) copy-start(f32[16,16,64]{1,2,0:T(8,128)} %copy.119) | copy-start | bytes 196612
  206.2 9.4 %copy-start.26 = (pred[16]{0:T(512)(128)(4,1)S(1)}, pred[16]{0:T(512)(128)(4,1)}, u32[]{:S(2)}) copy-start(pred[16]{0:T(512)(128)(4,1)} %get-tuple-element.77) | copy-start | bytes 52
  215.6 7.5 %copy-start.13 = (f32[16,1,16,64]{3,2,1,0:T(8,128)S(1)}, f32[16,1,16,64]{3,2,1,0:T(8,128)}, u32[]{:S(2)}) copy-start(f32[16,1,16,64]{3,2,1,0:T(8,128)} %get-tuple-element.36) | copy-start | bytes 196612
  223.1 9.3 %copy-start.12 = (f32[16,1,16,64]{3,2,1,0:T(8,128)S(1)}, f32[16,1,16,64]{3,2,1,0:T(8,128)}, u32[]{:S(2)}) copy-start(f32[16,1,16,64]{3,2,1,0:T(8,128)} %get-tuple-element.35) | copy-start | bytes 196612
  223.1 18.8 %copy-start.28 = (pred[16]{0:T(512)(128)(4,1)S(1)}, pred[16]{0:T(512)(128)(4,1)}, u32[]{:S(2)}) copy-start(pred[16]{0:T(512)(128)(4,1)} %get-tuple-element.79) | copy-start | bytes 52
  232.4 10.5 %copy-start.25 = (f32[1024]{0:T(1024)S(1)}, f32[1024]{0:T(1024)}, u32[]{:S(2)}) copy-start(f32[1024]{0:T(1024)} %mul.482) | copy-start | bytes 12292
  232.4 10.5 %copy-start.33 = (f32[64]{0:T(128)S(1)}, f32[64]{0:T(128)}, u32[]{:S(2)}) copy-start(f32[64]{0:T(128)} %copy-done.32) | copy-start | bytes 772
  232.4 21.3 %copy-start.7 = (bf16[64,4,1024]{2,1,0:T(4,128)(2,1)S(1)}, bf16[64,4,1024]{2,1,0:T(4,128)(2,1)}, u32[]{:S(2)}) copy-start(bf16[64,4,1024]{2,1,0:T(4,128)(2,1)} %param.15) | copy-start | bytes 1572868
  232.4 60.2 %copy-start.34 = (f32[1,1024]{1,0:T(1,128)S(1)}, f32[1,1024]{1,0:T(1,128)}, u32[]{:S(2)}) copy-start(f32[1,1024]{1,0:T(1,128)} %get-tuple-element.64) | copy-start | bytes 12292
  253.6 69.7 %reduce-scatter.47.cloned.1.call-start = ((), (), s32[]{:S(2)}) async-start(), calls=%async_computation.26 | async-start | bytes 81920
  292.6 27.5 %copy-start = (bf16[256,1024]{1,0:T(8,128)(2,1)}, bf16[256,1024]{1,0:T(8,128)(2,1)S(1)}, u32[]{:S(2)}) copy-start(bf16[256,1024]{1,0:T(8,128)(2,1)S(1)} %all_gather.13) | copy-start | bytes 1572868
  292.6 13.3 %copy-start.38 = (f32[64]{0:T(128)S(1)}, f32[64]{0:T(128)}, u32[]{:S(2)}) copy-start(f32[64]{0:T(128)} %get-tuple-element.70) | copy-start | bytes 772
  294.5 40.0 %reduce-scatter.49.cloned.1.call-start = ((), (), s32[]{:S(2)}) async-start(), calls=%async_computation.27 | async-start | bytes 81920
  296.3 62.2 %reduce-scatter.33.cloned.1.call-start = ((), (), s32[]{:S(2)}) async-start(), calls=%async_computation.19 | async-start | bytes 655360 | tf_op jit(solution)/shard_map/reduce_scatter | solution.py:101
  299.5 83.2 %reduce-scatter.35.cloned.1.call-start = ((), (), s32[]{:S(2)}) async-start(), calls=%async_computation.20 | async-start | bytes 655360 | tf_op jit(solution)/shard_map/reduce_scatter | solution.py:101
  302.7 104.0 %reduce-scatter.37.cloned.1.call-start = ((), (), s32[]{:S(2)}) async-start(), calls=%async_computation.21 | async-start | bytes 655360 | tf_op jit(solution)/shard_map/reduce_scatter | solution.py:101
  305.9 213.7 %reduce-scatter.39.cloned.1.call-start = ((), (), s32[]{:S(2)}) async-start(), calls=%async_computation.22 | async-start | bytes 655360 | tf_op jit(solution)/shard_map/reduce_scatter | solution.py:101
  306.6 29.5 %copy-start.35 = (f32[16]{0:T(128)S(1)}, f32[16]{0:T(128)}, u32[]{:S(2)}) copy-start(f32[16]{0:T(128)} %get-tuple-element.66) | copy-start | bytes 196
  306.6 29.5 %copy-start.36 = (f32[16]{0:T(128)S(1)}, f32[16]{0:T(128)}, u32[]{:S(2)}) copy-start(f32[16]{0:T(128)} %get-tuple-element.68) | copy-start | bytes 196
  320.1 86.6 %copy-start.30 = (f32[64]{0:T(128)}, f32[64]{0:T(128)S(1)}, u32[]{:S(2)}) copy-start(f32[64]{0:T(128)S(1)} %dynamic_slice.41) | copy-start | bytes 772
  323.2 230.9 %reduce-scatter.41.cloned.1.call-start = ((), (), s32[]{:S(2)}) async-start(), calls=%async_computation.23 | async-start | bytes 655360 | tf_op jit(solution)/shard_map/reduce_scatter | solution.py:136
  408.2 34.5 %copy-start.5 = (f32[16,4,16,64]{3,2,1,0:T(8,128)}, f32[16,4,16,64]{3,2,1,0:T(8,128)S(1)}, u32[]{:S(2)}) copy-start(f32[16,4,16,64]{3,2,1,0:T(8,128)S(1)} %reshape.245) | copy-start | bytes 786436
  408.8 17.4 %copy-start.23 = (pred[16]{0:T(512)(128)(4,1)S(1)}, pred[16]{0:T(512)(128)(4,1)}, u32[]{:S(2)}) copy-start(pred[16]{0:T(512)(128)(4,1)} %copy-done.21) | copy-start | bytes 52
  426.2 17.2 %slice-start = ((s8[8388608]{0:T(1024)(128)(4,1)}), s8[4194304]{0:T(1024)(128)(4,1)S(1)}, s32[]{:S(2)}) async-start(s8[8388608]{0:T(1024)(128)(4,1)} %bitcast.386), calls=%async_computation.28 | async-start | bytes 8388608
  426.3 17.2 %slice-start.1 = ((s8[8388608]{0:T(1024)(128)(4,1)}), s8[4194304]{0:T(1024)(128)(4,1)S(1)}, s32[]{:S(2)}) async-start(s8[8388608]{0:T(1024)(128)(4,1)} %bitcast.386), calls=%async_computation.29 | async-start | bytes 8388608
  433.4 10.1 %copy-start.29 = (pred[16]{0:T(512)(128)(4,1)S(1)}, pred[16]{0:T(512)(128)(4,1)}, u32[]{:S(2)}) copy-start(pred[16]{0:T(512)(128)(4,1)} %get-tuple-element.79) | copy-start | bytes 52
  450.3 10.3 %copy-start.11 = (f32[16,1,16,64]{3,2,1,0:T(8,128)S(1)}, f32[16,1,16,64]{3,2,1,0:T(8,128)}, u32[]{:S(2)}) copy-start(f32[16,1,16,64]{3,2,1,0:T(8,128)} %get-tuple-element.26) | copy-start | bytes 196612
  450.3 20.0 %copy-start.6 = (f32[16,4,16,64]{3,2,1,0:T(8,128)S(1)}, f32[16,4,16,64]{3,2,1,0:T(8,128)}, u32[]{:S(2)}) copy-start(f32[16,4,16,64]{3,2,1,0:T(8,128)} %copy-done.5) | copy-start | bytes 786436
  450.3 20.0 %copy-start.20 = (f32[16,1,16]{2,1,0:T(1,128)S(1)}, f32[16,1,16]{2,1,0:T(1,128)}, u32[]{:S(2)}) copy-start(f32[16,1,16]{2,1,0:T(1,128)} %get-tuple-element.49) | copy-start | bytes 3076
  450.3 20.1 %copy-start.17 = (f32[16,1,16,64]{3,2,1,0:T(8,128)S(1)}, f32[16,1,16,64]{3,2,1,0:T(8,128)}, u32[]{:S(2)}) copy-start(f32[16,1,16,64]{3,2,1,0:T(8,128)} %get-tuple-element.25) | copy-start | bytes 196612
  479.9 2.9 copy-start.9
  482.8 9.4 %copy-start.2 = (f32[16,16,64]{1,2,0:T(8,128)S(1)}, f32[16,16,64]{1,2,0:T(8,128)}, u32[]{:S(2)}) copy-start(f32[16,16,64]{1,2,0:T(8,128)} %copy.130) | copy-start | bytes 196612
  482.8 9.4 %copy-start.27 = (pred[16]{0:T(512)(128)(4,1)S(1)}, pred[16]{0:T(512)(128)(4,1)}, u32[]{:S(2)}) copy-start(pred[16]{0:T(512)(128)(4,1)} %get-tuple-element.77) | copy-start | bytes 52
  492.3 7.6 %copy-start.15 = (f32[16,1,16,64]{3,2,1,0:T(8,128)S(1)}, f32[16,1,16,64]{3,2,1,0:T(8,128)}, u32[]{:S(2)}) copy-start(f32[16,1,16,64]{3,2,1,0:T(8,128)} %get-tuple-element.24) | copy-start | bytes 196612
  499.8 9.3 %copy-start.14 = (f32[16,1,16,64]{3,2,1,0:T(8,128)S(1)}, f32[16,1,16,64]{3,2,1,0:T(8,128)}, u32[]{:S(2)}) copy-start(f32[16,1,16,64]{3,2,1,0:T(8,128)} %get-tuple-element.23) | copy-start | bytes 196612
  509.1 10.4 %copy-start.24 = (f32[1024]{0:T(1024)S(1)}, f32[1024]{0:T(1024)}, u32[]{:S(2)}) copy-start(f32[1024]{0:T(1024)} %mul.537) | copy-start | bytes 12292
  509.2 10.4 %copy-start.31 = (f32[64]{0:T(128)S(1)}, f32[64]{0:T(128)}, u32[]{:S(2)}) copy-start(f32[64]{0:T(128)} %copy-done.30) | copy-start | bytes 772
Sparse Core Ops, SparseCore 0:
  13.4 22.2 reduce-scatter.42
  38.2 19.5 reduce-scatter.44
  60.3 21.6 reduce-scatter.26
  84.3 21.6 reduce-scatter.24
  108.3 21.6 reduce-scatter.22
  132.9 21.6 reduce-scatter.28
  253.7 22.4 reduce-scatter.30
  294.6 17.8 reduce-scatter.46
  314.9 19.5 reduce-scatter.48
  336.8 21.6 reduce-scatter.32
  361.0 21.6 reduce-scatter.34
  385.0 21.6 reduce-scatter.36
  409.8 21.6 reduce-scatter.38
  530.4 22.4 reduce-scatter.40
where the time goes:
time: 585 us; the launch traced here: 579 us
  matrix products  192 us (33%)
  waiting for transfers between devices  159 us (27%)
  other arithmetic  88.5 us (15%)
  local copies, waits for them, and re-layouts  63.8 us (11%)
  blocking collectives  59.3 us (10%)
  between operations  15.1 us (3%)
    reduce_scatter x8, waiting for transfers between devices, body(): lax.psum_scatter(shortened(terms), 'dp', scatter_dimension=0, tiled=True)  126 us
    dot_general x8, matrix products, recur(): jnp.einsum('skhe,shk->she', decayed, keyvec[:, step], precision=lax.Preci...  81.8 us
    dot_general x8, matrix products, recur(): jnp.einsum('skhe,shk->she', updated, query[:, step], precision=lax.Precis...  76.9 us
    mul x8, other arithmetic, recur(): decayed = state * jnp.exp(fading_multiplier[:, step])[:, None, :, None]  48.6 us
    all_gather x2, blocking collectives, body(): resid = lax.all_gather(updated_rows, 'tp', axis=0, tiled=True)  31.6 us
    dot_general x12, matrix products, body(): jnp.dot(scaled, weight, preferred_element_type=jnp.float32)  27.4 us
    reduce_scatter x2, waiting for transfers between devices, body(): lax.psum_scatter(mixed_terms.astype(jnp.bfloat16), 'tp', scatter_dimensio...  22.4 us
    another operation x2, local copies, waits for them, and re-layouts, body(): return (resid.reshape(all_seqs, slots, feat), jnp.stack(fresh_states))  15.3 us
  transfers between devices with their start and end apart: 14, of which 9 were waited for; matrix products, arithmetic and copies ran while one was open for 56% of the time, Pallas kernels for 0%

commit v1 on v0

v1 whole, which is shorter than its diff:
```python
import functools

import jax
import jax.numpy as jnp
from jax import lax
from jax.experimental import pallas as pl
from jax.experimental.pallas import tpu as pltpu
from jax.sharding import PartitionSpec as P

BLOCKS = 2
EPS = 1e-06
F32 = jnp.float32
BF16 = jnp.bfloat16
MESH = pl.DeviceIdType.MESH
VMEM = pl.BlockSpec(memory_space=pltpu.VMEM)


def greet(axis, peers):
    barrier = pltpu.get_barrier_semaphore()
    for peer in peers:
        pl.semaphore_signal(barrier, inc=1, device_id={axis: peer}, device_id_type=MESH)
    pl.semaphore_wait(barrier, len(peers))


def send(src, dst, send_sem, recv_sem, axis, peer):
    copy = pltpu.make_async_remote_copy(
        src_ref=src,
        dst_ref=dst,
        send_sem=send_sem,
        recv_sem=recv_sem,
        device_id={axis: peer},
        device_id_type=MESH,
    )
    copy.start()
    return copy


def params(cid):
    return pltpu.CompilerParams(
        collective_id=cid, has_side_effects=True, vmem_limit_bytes=48 * 1024 * 1024
    )


def gather_kernel(n, x_ref, o_ref, land, send_sem, recv_sem):
    me = lax.axis_index("dp")
    peers = [lax.rem(me + d, n) for d in range(1, n)]
    greet("dp", peers)
    copies = [
        send(x_ref, land.at[me], send_sem.at[d], recv_sem.at[d], "dp", peer)
        for d, peer in enumerate(peers)
    ]
    for copy in copies:
        copy.wait()
    o_ref[...] = land[...]
    o_ref[me] = x_ref[...]


def gather_counts(counts, n, cid):
    own = counts.shape[0]
    block = jnp.broadcast_to(jnp.pad(counts, (0, 128 - own))[None, :], (8, 128))
    out = pl.pallas_call(
        functools.partial(gather_kernel, n),
        out_shape=jax.ShapeDtypeStruct((n, 8, 128), jnp.int32),
        in_specs=[VMEM],
        out_specs=VMEM,
        scratch_shapes=[
            pltpu.VMEM((n, 8, 128), jnp.int32),
            pltpu.SemaphoreType.DMA((n - 1,)),
            pltpu.SemaphoreType.DMA((n - 1,)),
        ],
        compiler_params=params(cid),
        name="gather_counts",
    )(block)
    return out[:, 0, :own].reshape(n * own)


def reduce_over_dp(n, x_refs, o_refs, scratch, sems):
    me = lax.axis_index("dp")
    chips = n // 2
    core = lax.rem(me, 2)
    partner = me + 1 - 2 * core
    others = [lax.rem(me + 2 * d, n) for d in range(1, chips)]
    greet("dp", [partner] + others)
    send_sem, recv_sem = sems
    width = chips + 1
    rows = x_refs[0].shape[0] // 2
    mine = pl.multiple_of(core * rows, 16)
    theirs = pl.multiple_of((1 - core) * rows, 16)
    first = []
    for a, x in enumerate(x_refs):
        half = scratch[a][0]
        first.append(
            send(x.at[pl.ds(theirs, rows)], half, send_sem.at[a * width], recv_sem.at[a * width], "dp", partner)
        )
    second = []
    for a, x in enumerate(x_refs):
        half, own, land, back = scratch[a]
        first[a].wait()
        for r in range(0, rows, 16):
            chunk = x[pl.ds(pl.multiple_of(mine + r, 16), 16), :].astype(F32) + half[pl.ds(r, 16), :].astype(F32)
            own[pl.ds(r, 16), :] = chunk.astype(BF16)
        second.append(
            [
                send(own, land.at[d], send_sem.at[a * width + 1 + d], recv_sem.at[a * width + 1 + d], "dp", peer)
                for d, peer in enumerate(others)
            ]
        )
    third = []
    for a, o in enumerate(o_refs):
        half, own, land, back = scratch[a]
        for copy in second[a]:
            copy.wait()
        for r in range(0, rows, 16):
            total = own[pl.ds(r, 16), :].astype(F32)
            for d in range(chips - 1):
                total = total + land[d, pl.ds(r, 16), :].astype(F32)
            own[pl.ds(r, 16), :] = total.astype(BF16)
        slot = a * width + chips
        third.append(send(own, back, send_sem.at[slot], recv_sem.at[slot], "dp", partner))
    for a, o in enumerate(o_refs):
        half, own, land, back = scratch[a]
        o[pl.ds(mine, rows), :] = own[...]
        third[a].wait()
        o[pl.ds(theirs, rows), :] = back[...]


def reduce_scratch(n, shapes):
    out = []
    for rows, cols in shapes:
        half = (rows // 2, cols)
        out += [
            pltpu.VMEM(half, BF16),
            pltpu.VMEM(half, BF16),
            pltpu.VMEM((n // 2 - 1,) + half, BF16),
            pltpu.VMEM(half, BF16),
        ]
    count = len(shapes) * (n // 2 + 1)
    return out + [pltpu.SemaphoreType.DMA((count,)), pltpu.SemaphoreType.DMA((count,))]


def dp_kernel(n, main, small, out_main, out_small, *rest):
    scratch = [rest[0:4], rest[4:8]]
    reduce_over_dp(n, [main, small], [out_main, out_small], scratch, rest[8:10])


def sum_projections(main, small, n, cid):
    shapes = [main.shape, small.shape]
    return pl.pallas_call(
        functools.partial(dp_kernel, n),
        out_shape=[jax.ShapeDtypeStruct(s, BF16) for s in shapes],
        in_specs=[VMEM, VMEM],
        out_specs=[VMEM, VMEM],
        scratch_shapes=reduce_scratch(n, shapes),
        compiler_params=params(cid),
        name="sum_projections",
    )(main, small)


def proj_kernel(where, h, gain, wq, wk, wv, wz, wa, wb, main, small, scaled):
    @pl.when(pl.program_id(0) == 0)
    def _():
        rows = h[...]
        bent = (rows * gain[...].astype(F32)).astype(BF16)
        scaled[...] = bent
        heads = wa.shape[2]
        both = jnp.concatenate([wa[0], wb[0]], axis=1)
        small[:, : 2 * heads] = jnp.dot(bent, both, preferred_element_type=F32).astype(BF16)
        squares = jnp.sum(rows * rows, axis=1, keepdims=True)
        rest = small.shape[1] - 2 * heads
        small[:, 2 * heads :] = jnp.broadcast_to(squares, (rows.shape[0], rest)).astype(BF16)

    tile = wq.shape[2]
    for i, w in enumerate((wq, wk, wv, wz)):
        main[:, i * tile : (i + 1) * tile] = jnp.dot(
            scaled[...], w[0], preferred_element_type=F32
        ).astype(BF16)


def project(h, gain, weights, wa, wb, layer, where):
    rows, feat = h.shape
    cols = weights[0].shape[2]
    tile = min(256, cols)
    heads = wa.shape[2]
    wide = pl.BlockSpec((1, feat, tile), lambda j, s: (layer, 0, j))
    thin = pl.BlockSpec((1, feat, heads), lambda j, s: (layer, s[0], 0))
    return pl.pallas_call(
        proj_kernel,
        out_shape=[
            jax.ShapeDtypeStruct((rows, 4 * cols), BF16),
            jax.ShapeDtypeStruct((rows, 2 * heads + 128), BF16),
        ],
        grid_spec=pltpu.PrefetchScalarGridSpec(
            num_scalar_prefetch=1,
            grid=(cols // tile,),
            in_specs=[
                pl.BlockSpec((rows, feat), lambda j, s: (0, 0)),
                pl.BlockSpec((1, feat), lambda j, s: (0, 0)),
                wide, wide, wide, wide, thin, thin,
            ],
            out_specs=[
                pl.BlockSpec((rows, 4 * tile), lambda j, s: (0, j)),
                pl.BlockSpec((rows, 2 * heads + 128), lambda j, s: (0, 0)),
            ],
            scratch_shapes=[pltpu.VMEM((rows, feat), BF16)],
        ),
        name="project",
    )(where, h, gain, *weights, wa, wb)


def recur_kernel(
    width, size, head_size, heads_all, counts, where, main, small, pos_col, pos_row, speed, bias,
    shrink, gain, state, carried, y, new, q_s, k_s, v_s, z_s, dec_s, beta_s, o_s,
):
    seq = pl.program_id(0)
    slots = q_s.shape[0] // pl.num_programs(0)
    tile = min(256, q_s.shape[1])
    cols = q_s.shape[1]
    row = lax.broadcasted_iota(jnp.int32, (tile, tile), 0) // head_size
    col = lax.broadcasted_iota(jnp.int32, (tile, tile), 1) // head_size
    blocks = (row == col).astype(BF16)

    @pl.when(seq == 0)
    def _():
        own = q_s.shape[0]
        packed = main.shape[0]
        pick = (pos_col[...] == lax.broadcasted_iota(jnp.int32, (own, packed), 1)).astype(BF16)
        few = jnp.dot(pick, small[...], preferred_element_type=F32)
        factor = lax.rsqrt(few[:, 2 * heads_all : 2 * heads_all + 1] / width + EPS)
        heads = speed.shape[1]
        first = where[1] * heads
        ones = lax.broadcasted_iota(jnp.int32, (heads_all, cols), 0)
        lane = lax.broadcasted_iota(jnp.int32, (heads_all, cols), 1) // head_size
        spread_all = (ones == lane + first).astype(BF16)
        spread = (
            lax.broadcasted_iota(jnp.int32, (heads, cols), 0)
            == lax.broadcasted_iota(jnp.int32, (heads, cols), 1) // head_size
        ).astype(F32)
        pa = jnp.dot(few[:, :heads_all].astype(BF16), spread_all, preferred_element_type=F32) * factor
        pb = jnp.dot(
            few[:, heads_all : 2 * heads_all].astype(BF16), spread_all, preferred_element_type=F32
        ) * factor
        exact = functools.partial(
            jnp.dot, precision=lax.Precision.HIGHEST, preferred_element_type=F32
        )
        rate = exact(jnp.broadcast_to(jnp.exp(speed[...]), (8, heads)), spread)[:1]
        offset = exact(jnp.broadcast_to(bias[...], (8, heads)), spread)[:1]
        extra = exact(shrink[...], spread)
        arg = pa + offset
        soft = jnp.maximum(arg, 0.0) + jnp.log1p(jnp.exp(-jnp.abs(arg)))
        dec_s[...] = jnp.exp(extra - rate * soft)
        beta_s[...] = jax.nn.sigmoid(pb)
        for j in range(cols // tile):
            here = slice(j * tile, (j + 1) * tile)
            chunk = jnp.dot(
                pick, main[:, j * 4 * tile : (j + 1) * 4 * tile], preferred_element_type=F32
            ) * factor
            for i, dst in enumerate((q_s, k_s, v_s, z_s)):
                val = chunk[:, i * tile : (i + 1) * tile]
                val = val * jax.nn.sigmoid(val)
                if i < 2:
                    total = jnp.dot((val * val).astype(BF16), blocks, preferred_element_type=F32)
                    val = val * lax.rsqrt(total + EPS)
                    if i == 0:
                        val = val * head_size ** (-0.5)
                dst[:, here] = val
        o_s[...] = jnp.zeros_like(o_s)

    new[...] = state[...]
    key_row = lax.broadcasted_iota(jnp.int32, (size, tile), 0)
    key_col = lax.rem(lax.broadcasted_iota(jnp.int32, (size, tile), 1), head_size)
    diag = key_row == key_col
    count = counts[seq]
    for t in range(slots):

        @pl.when(t < count)
        def _():
            at = pl.ds(seq * slots + t, 1)
            for j in range(cols // tile):
                here = slice(j * tile, (j + 1) * tile)
                kq = jnp.concatenate(
                    [
                        jnp.where(diag, jnp.broadcast_to(k_s[at, here], (size, tile)), 0.0),
                        jnp.where(diag, jnp.broadcast_to(q_s[at, here], (size, tile)), 0.0),
                    ],
                    axis=0,
                ).astype(BF16)
                kq = jnp.dot(kq, blocks, preferred_element_type=F32)
                kmat, qmat = kq[:size], kq[size:]
                decayed = new[0, 0, :, here] * dec_s[at, here]
                guess = jnp.sum(decayed * kmat, axis=0, keepdims=True)
                fresh = beta_s[at, here] * (v_s[at, here] - guess)
                updated = decayed + kmat * fresh
                new[0, 0, :, here] = updated
                o_s[at, here] = jnp.sum(updated * qmat, axis=0, keepdims=True)

    @pl.when(seq == pl.num_programs(0) - 1)
    def _():
        own = q_s.shape[0]
        packed = main.shape[0]
        place = (lax.broadcasted_iota(jnp.int32, (packed, own), 0) == pos_row[...]).astype(BF16)
        for j in range(cols // tile):
            here = slice(j * tile, (j + 1) * tile)
            val = o_s[:, here]
            total = jnp.dot((val * val).astype(BF16), blocks, preferred_element_type=F32)
            val = val * lax.rsqrt(total / head_size + EPS) * gain[:, here] * z_s[:, here]
            y[:, here] = jnp.dot(place, val.astype(BF16), preferred_element_type=F32).astype(BF16)


def recur(counts, where, main, small, pos, speed, bias, shrink, gain, states, carried, layer, width, heads_all):
    own_seqs = counts.shape[0]
    packed = main.shape[0]
    size, cols = states.shape[2:]
    own = pos.shape[0]
    heads = speed.shape[1]
    whole = lambda shape: pl.BlockSpec(shape, lambda s, *_: (0,) * len(shape))
    here = pl.BlockSpec((1, 1, size, cols), lambda s, *_: (layer, s, 0, 0))
    args = [main, small, pos[:, None], pos[None, :], speed, bias, shrink, gain]
    specs = [whole(a.shape) for a in args] + [here]
    kernel = functools.partial(recur_kernel, width, size, cols // heads, heads_all)
    if carried is None:
        body = lambda *refs: kernel(*refs[:11], None, *refs[11:])
        more, alias = [], {}
    else:
        body = kernel
        more, alias = [carried], {11: 1}
        specs = specs + [pl.BlockSpec(memory_space=pl.ANY)]
    return pl.pallas_call(
        body,
        out_shape=[
            jax.ShapeDtypeStruct((packed, cols), BF16),
            jax.ShapeDtypeStruct(states.shape, F32),
        ],
        grid_spec=pltpu.PrefetchScalarGridSpec(
            num_scalar_prefetch=2,
            grid=(own_seqs,),
            in_specs=specs,
            out_specs=[whole((packed, cols)), here],
            scratch_shapes=[pltpu.VMEM((own, cols), F32) for _ in range(7)],
        ),
        input_output_aliases=alias,
        name="recur",
    )(counts, where, *args, states, *more)


def gated_kernel(n, y, out, *rest):
    reduce_over_dp(n, [y], [out], [rest[0:4]], rest[4:6])


def share_gated(y, n, cid):
    return pl.pallas_call(
        functools.partial(gated_kernel, n),
        out_shape=jax.ShapeDtypeStruct(y.shape, BF16),
        in_specs=[VMEM],
        out_specs=VMEM,
        scratch_shapes=reduce_scratch(n, [y.shape]),
        compiler_params=params(cid),
        name="share_gated",
    )(y)


def mix_kernel(m, gated, w, h, out, part, land, own, gath, send_a, recv_a, send_b, recv_b):
    me = lax.axis_index("tp")
    peers = [lax.rem(me + d, m) for d in range(1, m)]
    greet("tp", peers)
    rows = part.shape[1]
    mixed = jnp.dot(gated[...], w[0], preferred_element_type=F32)
    for j in range(m):
        part[j] = mixed[j * rows : (j + 1) * rows].astype(BF16)
    copies = [
        send(part.at[peer], land.at[d], send_a.at[d], recv_a.at[d], "tp", peer)
        for d, peer in enumerate(peers)
    ]
    total = part[me].astype(F32)
    for d, copy in enumerate(copies):
        copy.wait()
        total = total + land[d].astype(F32)
    own[...] = total.astype(BF16)
    copies = [
        send(own, gath.at[me], send_b.at[d], recv_b.at[d], "tp", peer)
        for d, peer in enumerate(peers)
    ]
    for copy in copies:
        copy.wait()
    gath[me] = own[...]
    for j in range(m):
        at = slice(j * rows, (j + 1) * rows)
        out[at, :] = (h[at, :] + gath[j].astype(F32)).astype(BF16).astype(F32)


def mix(gated, w, h, layer, m, cid):
    packed, feat = h.shape
    cols = gated.shape[1]
    rows = packed // m
    once = lambda shape: pl.BlockSpec(shape, lambda i: (0,) * len(shape))
    return pl.pallas_call(
        functools.partial(mix_kernel, m),
        grid=(1,),
        out_shape=jax.ShapeDtypeStruct(h.shape, F32),
        in_specs=[
            once(gated.shape),
            pl.BlockSpec((1, cols, feat), lambda i: (layer, 0, 0)),
            once(h.shape),
        ],
        out_specs=once(h.shape),
        scratch_shapes=[
            pltpu.VMEM((m, rows, feat), BF16),
            pltpu.VMEM((m - 1, rows, feat), BF16),
            pltpu.VMEM((rows, feat), BF16),
            pltpu.VMEM((m, rows, feat), BF16),
            *[pltpu.SemaphoreType.DMA((m - 1,)) for _ in range(4)],
        ],
        compiler_params=params(cid),
        name="mix",
    )(gated, w, h)


def body(
    n,
    m,
    resid,
    counts,
    wq,
    wk,
    wv,
    wz,
    wa,
    wb,
    wo,
    speed,
    bias,
    scaling,
    channel,
    shrink,
    states,
):
    all_seqs, slots, feat = resid.shape
    own_seqs = counts.shape[0]
    own = own_seqs * slots
    heads = speed.shape[1]
    live_rows = all_seqs * 3 // 2
    step = -(-live_rows // m)
    step = -(-step // 8) * 8
    while step * m % 32:
        step += 8
    packed = step * m
    dp = lax.axis_index("dp")
    where = jnp.stack([dp, lax.axis_index("tp")]).astype(jnp.int32)
    every = gather_counts(counts, n, 1)
    before = lax.broadcasted_iota(jnp.int32, (all_seqs, all_seqs), 1) < lax.broadcasted_iota(
        jnp.int32, (all_seqs, all_seqs), 0
    )
    start = jnp.sum(jnp.where(before, every[None, :], 0), axis=1)
    slot = lax.broadcasted_iota(jnp.int32, (all_seqs, slots), 1)
    pos = jnp.where(slot < every[:, None], start[:, None] + slot, -1).reshape(all_seqs * slots)
    pos_own = lax.dynamic_slice_in_dim(pos, dp * own, own, 0)
    onehot = (lax.broadcasted_iota(jnp.int32, (packed, all_seqs * slots), 0) == pos[None, :]).astype(BF16)
    flat = resid.reshape(all_seqs * slots, feat)
    h = jnp.dot(onehot, flat, preferred_element_type=F32)
    carried = None
    for l in range(BLOCKS):
        main, small = project(h, scaling[l][None], (wq, wk, wv, wz), wa, wb, l, where)
        main, small = sum_projections(main, small, n, 2 + 3 * l)
        gain = jnp.tile(channel[l].astype(F32), heads)[None]
        y, carried = recur(
            counts, where, main, small, pos_own, speed[l][None], bias[l][None],
            shrink[l].reshape(own, heads), gain, states, carried, l, feat * n, wa.shape[2],
        )
        gated = share_gated(y, n, 3 + 3 * l)
        h = mix(gated, wo, h, l, m, 4 + 3 * l)
    back = lax.dot_general(
        onehot, h.astype(BF16), (((0,), (0,)), ((), ())), preferred_element_type=F32
    )
    out = jnp.where(pos[:, None] >= 0, back, flat.astype(F32)).astype(BF16)
    return out.reshape(all_seqs, slots, feat), carried


def solution(mesh):
    in_specs = (
        P("grp", None, "dp"),
        P(("grp", "dp")),
        P(None, "dp", "tp"),
        P(None, "dp", "tp"),
        P(None, "dp", "tp"),
        P(None, "dp", "tp"),
        P(),
        P(),
        P(None, "tp", "dp"),
        P(None, "tp"),
        P(None, "tp"),
        P(None, "dp"),
        P(),
        P(None, ("grp", "dp"), None, "tp"),
        P(None, ("grp", "dp"), None, "tp"),
    )
    out_specs = (P("grp", None, "dp"), P(None, ("grp", "dp"), None, "tp"))
    run = functools.partial(body, mesh.shape["dp"], mesh.shape["tp"])
    return jax.shard_map(run, mesh=mesh, in_specs=in_specs, out_specs=out_specs, check_vma=False)
```

time: 585 us -> 159 us (0.27)
  matrix products: 192 us -> 1.31 us
  waiting for transfers between devices: 159 us -> 0 us
  Pallas kernels: 0 us -> 129 us
  other arithmetic: 88.5 us -> 0.85 us
  blocking collectives: 59.3 us -> 0 us
  local copies, waits for them, and re-layouts: 63.8 us -> 25.9 us
  between operations: 15.1 us -> 0.82 us
    dot_general x30 -> x2, matrix products: 192 us -> 1.31 us  [the longest x1 0.97 us: body(): h = jnp.dot(onehot, flat, preferred_element_type=F32)]
    reduce_scatter x10 -> x0, waiting for transfers between devices: 148 us -> none  [the longest x8 126 us: body(): lax.psum_scatter(shortened(terms), 'dp', scatter_dimension=0, tiled=True)]
    pallas_call x0 -> x11, Pallas kernels: none -> 129 us  [the longest x2 35.5 us: recur(): pl.pallas_call(body, out_shape=[jax.ShapeDtypeStruct((packed, cols), BF16...]
    mul x25 -> x0, other arithmetic: 55.9 us -> none  [the longest x8 48.6 us: recur(): decayed = state * jnp.exp(fading_multiplier[:, step])[:, None, :, None]]
    all_gather x4 -> x0, blocking collectives: 44.6 us -> none  [the longest x2 31.6 us: body(): resid = lax.all_gather(updated_rows, 'tp', axis=0, tiled=True)]
    another operation x4, local copies, waits for them, and re-layouts: 29.9 us -> 1.35 us  [body(): gain = jnp.tile(channel[l].astype(F32), heads)[None]]
    slice x9 -> x4, local copies, waits for them, and re-layouts: 17 us -> 1.84 us  [the longest x1 0.62 us: body(): shrink[l].reshape(own, heads)]
    select_n x2 -> x1, other arithmetic: 15 us -> 0.09 us  [body(): jnp.where(slot < every[:, None], start[:, None] + slot, -1)]
  transfers between devices with their start and end apart: 14 -> 0, of which waited for: 9 -> 0; matrix products, arithmetic and copies ran while one was open for 56% -> 0% of each run, Pallas kernels for 0% -> 0%
where the time goes in v1:
time: 159 us; the launch traced here: 158 us
  Pallas kernels  129 us (81%)
  local copies, waits for them, and re-layouts  25.9 us (16%)
    pallas_call x2, Pallas kernels, recur(): pl.pallas_call(body, out_shape=[jax.ShapeDtypeStruct((packed, cols), BF16...  35.5 us
    pallas_call x2, Pallas kernels, sum_projections(): pl.pallas_call(functools.partial(dp_kernel, n), out_shape=[jax.ShapeDtype...  30.1 us
    pallas_call x2, Pallas kernels, mix(): pl.pallas_call(functools.partial(mix_kernel, m), grid=(1,), out_shape=jax...  28.8 us
    unnamed x44, local copies, waits for them, and re-layouts  18.3 us
    pallas_call x2, Pallas kernels, share_gated(): pl.pallas_call(functools.partial(gated_kernel, n), out_shape=jax.ShapeDty...  15.7 us
    pallas_call x2, Pallas kernels, project(): pl.pallas_call(proj_kernel, out_shape=[jax.ShapeDtypeStruct((rows, 4 * co...  14.3 us
    pallas_call x1, Pallas kernels, gather_counts(): pl.pallas_call(functools.partial(gather_kernel, n), out_shape=jax.ShapeDt...  4.61 us

profile of v1, /device:TPU:0, one launch (start us, length us, event | category | flops | bytes accessed | tf_op | source)
XLA Modules:
  0.0 157.9 jit_solution(4862912115882454101)
XLA Ops:
  0.6 0.0 copy-start.15
  0.6 0.0 copy-start.17
  0.6 0.7 pad.4
  1.4 4.6 %gather_counts.1 = s32[4,8,128]{2,1,0:T(8,128)S(1)} custom-call(s32[8,128]{1,0:T(8,128)S(1)} %broadcast_in_dim.39.x_ref), custom_call_target="tpu_custom_call" | custom-call | tf_op jit(solution)/shard_map/gather_counts/pallas_call | solution.py:61
  6.0 0.1 lt.27
  6.1 0.1 select_reduce_fusion
  6.2 0.1 add_select_fusion
  6.3 0.1 select_n.30
  6.4 1.2 reshape.76
  7.6 1.0 fusion.2.h
  8.6 0.6 pad_add_fusion.where.refs_1_
  9.2 2.7 %copy.30.wa = bf16[2,4096,64]{2,1,0:T(8,128)(2,1)} copy(bf16[2,4096,64]{1,2,0:T(8,128)(2,1)} %param.21) | data formatting | bytes 2097152 | tf_op args[6]
  11.9 0.0 copy-done.15
  11.9 1.7 %copy.31.wb = bf16[2,4096,64]{2,1,0:T(8,128)(2,1)} copy(bf16[2,4096,64]{1,2,0:T(8,128)(2,1)S(1)} %copy-done.15) | data formatting | bytes 2097152 | tf_op args[7]
  13.7 0.0 copy-done.17
  13.7 0.6 fusion.6
  14.3 0.0 copy-start.19
  14.3 0.0 copy-start.20
  14.3 0.0 copy-start.16
  14.3 0.0 copy-start.18
  14.3 7.2 %project.2 = (bf16[96,4096]{1,0:T(8,128)(2,1)}, bf16[96,256]{1,0:T(8,128)(2,1)}) custom-call(s32[2]{0:T(128)} %pad_add_fusion.where.refs_1_, f32[96,1024]{1,0:T(8,128)} %fusion.2.h, bf16[1,1024]{1,0:T(2,128)(2,1)} %get-tuple-element.29.gain, bf16[2,1024,1024]{2,1,0:T(8,128)(2,1)} %wq.3, bf16[2,1024,1024]{2,1,0:T(8,128)(2,1)} %wk.3, ...), custom_call_target="tpu_custom_call" | custom-call | tf_op jit(solution)/shard_map/project/pallas_call | solution.py:186
  21.5 0.0 copy-start.7
  21.5 1.1 copy-done.7
  22.7 0.0 copy-start.13
  22.7 0.8 copy-done.13
  23.5 15.1 %sum_projections.2 = (bf16[96,4096]{1,0:T(8,128)(2,1)S(1)}, bf16[96,256]{1,0:T(8,128)(2,1)S(1)}) custom-call(bf16[96,4096]{1,0:T(8,128)(2,1)S(1)} %copy-done.7, bf16[96,256]{1,0:T(8,128)(2,1)S(1)} %copy-done.13), custom_call_target="tpu_custom_call" | custom-call | tf_op jit(solution)/shard_map/sum_projections/pallas_call | solution.py:148
  38.6 0.0 copy-start.5
  38.6 0.9 copy-done.5
  39.4 0.6 copy-done.11
  40.1 0.6 dynamic-slice_bitcast_fusion
  40.6 0.7 copy.32.refs_4_.pos_col
  41.3 0.0 copy-done.19
  41.3 0.0 copy-done.20
  41.3 0.6 fusion.7
  41.9 0.0 copy-done.16
  41.9 0.6 fusion.5
  42.6 0.0 copy-done.18
  42.6 0.7 broadcast_in_dim_tile.6.refs_9_
  43.3 17.8 %recur.2 = (bf16[96,1024]{1,0:T(8,128)(2,1)}, f32[2,16,64,1024]{3,2,1,0:T(8,128)}) custom-call(s32[16]{0:T(128)} %counts.1, s32[2]{0:T(128)} %pad_add_fusion.where.refs_1_, bf16[96,4096]{1,0:T(8,128)(2,1)} %copy-done.5, bf16[96,256]{1,0:T(8,128)(2,1)} %copy-done.11, s32[64,1]{1,0:T(8,128)} %copy.32.refs_4_.pos_col, ...), custom_call_target="tpu_custom_call" | custom-call | tf_op jit(solution)/shard_map/recur/pallas_call | solution.py:327
  61.0 0.9 copy-done.10
  61.9 7.9 %share_gated.2.gated = bf16[96,1024]{1,0:T(8,128)(2,1)S(1)} custom-call(bf16[96,1024]{1,0:T(8,128)(2,1)S(1)} %copy-done.10), custom_call_target="tpu_custom_call" | custom-call | tf_op jit(solution)/shard_map/share_gated/pallas_call | solution.py:350
  69.8 0.0 copy-done.4
  69.8 0.0 copy-start
  69.8 2.2 %copy-done = bf16[2,1024,1024]{2,1,0:T(8,128)(2,1)S(1)} copy-done((bf16[2,1024,1024]{2,1,0:T(8,128)(2,1)S(1)}, bf16[2,1024,1024]{2,1,0:T(8,128)(2,1)}, u32[]{:S(2)}) %copy-start) | copy-done | bytes 4194328
  72.0 14.5 %mix.2.h = f32[96,1024]{1,0:T(8,128)S(1)} custom-call(bf16[96,1024]{1,0:T(8,128)(2,1)S(1)} %share_gated.2.gated, bf16[2,1024,1024]{2,1,0:T(8,128)(2,1)S(1)} %copy-done, f32[96,1024]{1,0:T(8,128)S(1)} %copy-done.4), custom_call_target="tpu_custom_call" | custom-call | tf_op jit(solution)/shard_map/mix/pallas_call | solution.py:395
  86.6 0.0 copy-start.2
  86.6 0.7 copy-done.2
  87.3 7.1 %project.3 = (bf16[96,4096]{1,0:T(8,128)(2,1)}, bf16[96,256]{1,0:T(8,128)(2,1)}) custom-call(s32[2]{0:T(128)} %pad_add_fusion.where.refs_1_, f32[96,1024]{1,0:T(8,128)} %copy-done.2, bf16[1,1024]{1,0:T(2,128)(2,1)} %get-tuple-element.28.gain, bf16[2,1024,1024]{2,1,0:T(8,128)(2,1)} %wq.3, bf16[2,1024,1024]{2,1,0:T(8,128)(2,1)} %wk.3, ...), custom_call_target="tpu_custom_call" | custom-call | tf_op jit(solution)/shard_map/project/pallas_call | solution.py:186
  94.4 1.1 copy-done.6
  95.5 0.8 copy-done.12
  96.3 15.0 %sum_projections.3 = (bf16[96,4096]{1,0:T(8,128)(2,1)S(1)}, bf16[96,256]{1,0:T(8,128)(2,1)S(1)}) custom-call(bf16[96,4096]{1,0:T(8,128)(2,1)S(1)} %copy-done.6, bf16[96,256]{1,0:T(8,128)(2,1)S(1)} %copy-done.12), custom_call_target="tpu_custom_call" | custom-call | tf_op jit(solution)/shard_map/sum_projections/pallas_call | solution.py:148
  111.3 0.0 copy-start.8
  111.3 0.9 copy-done.8
  112.2 0.6 copy-done.14
  112.8 0.7 broadcast_in_dim_tile.7.gain
  113.5 17.8 %recur.3 = (bf16[96,1024]{1,0:T(8,128)(2,1)}, f32[2,16,64,1024]{3,2,1,0:T(8,128)}) custom-call(s32[16]{0:T(128)} %counts.1, s32[2]{0:T(128)} %pad_add_fusion.where.refs_1_, bf16[96,4096]{1,0:T(8,128)(2,1)} %copy-done.8, bf16[96,256]{1,0:T(8,128)(2,1)} %copy-done.14, s32[64,1]{1,0:T(8,128)} %copy.32.refs_4_.pos_col, ...), custom_call_target="tpu_custom_call", output_to_operand_aliasing={{1}: (11, {})} | custom-call | tf_op jit(solution)/shard_map/recur/pallas_call | solution.py:327
  131.2 0.9 copy-done.9
  132.2 7.9 %share_gated.3.gated = bf16[96,1024]{1,0:T(8,128)(2,1)S(1)} custom-call(bf16[96,1024]{1,0:T(8,128)(2,1)S(1)} %copy-done.9), custom_call_target="tpu_custom_call" | custom-call | tf_op jit(solution)/shard_map/share_gated/pallas_call | solution.py:350
  140.0 0.0 copy-done.3
  140.0 0.0 copy-start.1
  140.0 2.2 %copy-done.1 = bf16[2,1024,1024]{2,1,0:T(8,128)(2,1)S(1)} copy-done((bf16[2,1024,1024]{2,1,0:T(8,128)(2,1)S(1)}, bf16[2,1024,1024]{2,1,0:T(8,128)(2,1)}, u32[]{:S(2)}) %copy-start.1) | copy-done | bytes 4194328
  142.2 14.3 %mix.3 = f32[96,1024]{1,0:T(8,128)S(1)} custom-call(bf16[96,1024]{1,0:T(8,128)(2,1)S(1)} %share_gated.3.gated, bf16[2,1024,1024]{2,1,0:T(8,128)(2,1)S(1)} %copy-done.1, f32[96,1024]{1,0:T(8,128)S(1)} %copy-done.3), custom_call_target="tpu_custom_call" | custom-call | tf_op jit(solution)/shard_map/mix/pallas_call | solution.py:395
  156.5 0.3 fusion
  156.9 1.0 reshape.77
  (14 shorter events, 0.1 us)
Async XLA Ops:
  0.6 11.3 %copy-start.15 = (bf16[2,4096,64]{1,2,0:T(8,128)(2,1)S(1)}, bf16[2,4096,64]{1,2,0:T(8,128)(2,1)}, u32[]{:S(2)}) copy-start(bf16[2,4096,64]{1,2,0:T(8,128)(2,1)} %param.22) | copy-start | bytes 3145732
  0.6 13.1 %copy-start.17 = (bf16[2,1024]{1,0:T(2,128)(2,1)S(1)}, bf16[2,1024]{1,0:T(2,128)(2,1)}, u32[]{:S(2)}) copy-start(bf16[2,1024]{1,0:T(2,128)(2,1)} %param.26) | copy-start | bytes 12292
  14.3 27.0 %copy-start.19 = (f32[2,16]{1,0:T(2,128)S(1)}, f32[2,16]{1,0:T(2,128)}, u32[]{:S(2)}) copy-start(f32[2,16]{1,0:T(2,128)} %param.25) | copy-start | bytes 388
  14.3 27.1 %copy-start.20 = (f32[2,16]{1,0:T(2,128)S(1)}, f32[2,16]{1,0:T(2,128)}, u32[]{:S(2)}) copy-start(f32[2,16]{1,0:T(2,128)} %param.24) | copy-start | bytes 388
  14.3 27.6 %copy-start.16 = (f32[2,16,4,16]{3,2,1,0:T(4,128)S(1)}, f32[2,16,4,16]{3,2,1,0:T(4,128)}, u32[]{:S(2)}) copy-start(f32[2,16,4,16]{3,2,1,0:T(4,128)} %param.28) | copy-start | bytes 24580
  14.3 28.3 %copy-start.18 = (bf16[2,64]{1,0:T(2,128)(2,1)S(1)}, bf16[2,64]{1,0:T(2,128)(2,1)}, u32[]{:S(2)}) copy-start(bf16[2,64]{1,0:T(2,128)(2,1)} %param.27) | copy-start | bytes 772
  21.5 1.1 copy-start.7
  22.7 0.8 copy-start.13
  38.6 0.9 copy-start.5
  39.4 0.6 copy-start.11
  43.2 26.6 %copy-start.4 = (f32[96,1024]{1,0:T(8,128)S(1)}, f32[96,1024]{1,0:T(8,128)}, u32[]{:S(2)}) copy-start(f32[96,1024]{1,0:T(8,128)} %fusion.2.h) | copy-start | bytes 1179652
  61.0 0.9 copy-start.10
  69.8 2.2 %copy-start = (bf16[2,1024,1024]{2,1,0:T(8,128)(2,1)S(1)}, bf16[2,1024,1024]{2,1,0:T(8,128)(2,1)}, u32[]{:S(2)}) copy-start(bf16[2,1024,1024]{2,1,0:T(8,128)(2,1)} %w.3) | copy-start | bytes 12582916
  86.6 0.7 copy-start.2
  94.4 1.1 copy-start.6
  95.5 0.8 copy-start.12
  111.3 0.9 copy-start.8
  112.2 0.6 copy-start.14
  113.5 26.6 %copy-start.3 = (f32[96,1024]{1,0:T(8,128)S(1)}, f32[96,1024]{1,0:T(8,128)}, u32[]{:S(2)}) copy-start(f32[96,1024]{1,0:T(8,128)} %copy-done.2) | copy-start | bytes 1179652
  131.2 0.9 copy-start.9
  140.0 2.2 %copy-start.1 = (bf16[2,1024,1024]{2,1,0:T(8,128)(2,1)S(1)}, bf16[2,1024,1024]{2,1,0:T(8,128)(2,1)}, u32[]{:S(2)}) copy-start(bf16[2,1024,1024]{2,1,0:T(8,128)(2,1)} %w.3) | copy-start | bytes 12582916

commit v2 on v1

--- a/solution.py
+++ b/solution.py
@@ -74,26 +74,25 @@
     return out[:, 0, :own].reshape(n * own)
 
 
-def reduce_over_dp(n, x_refs, o_refs, scratch, sems):
+def dp_partners(n):
     me = lax.axis_index("dp")
-    chips = n // 2
     core = lax.rem(me, 2)
     partner = me + 1 - 2 * core
-    others = [lax.rem(me + 2 * d, n) for d in range(1, chips)]
-    greet("dp", [partner] + others)
+    return core, partner, [lax.rem(me + 2 * d, n) for d in range(1, n // 2)]
+
+
+def reduce_over_dp(n, produce, x_refs, store, scratch, sems):
+    chips = n // 2
+    core, partner, others = dp_partners(n)
     send_sem, recv_sem = sems
     width = chips + 1
     rows = x_refs[0].shape[0] // 2
     mine = pl.multiple_of(core * rows, 16)
     theirs = pl.multiple_of((1 - core) * rows, 16)
-    first = []
-    for a, x in enumerate(x_refs):
-        half = scratch[a][0]
-        first.append(
-            send(x.at[pl.ds(theirs, rows)], half, send_sem.at[a * width], recv_sem.at[a * width], "dp", partner)
-        )
-    second = []
-    for a, x in enumerate(x_refs):
+    first, second, third = [], [], []
+
+    def cross(a):
+        x = x_refs[a]
         half, own, land, back = scratch[a]
         first[a].wait()
         for r in range(0, rows, 16):
@@ -105,8 +104,19 @@
                 for d, peer in enumerate(others)
             ]
         )
-    third = []
-    for a, o in enumerate(o_refs):
+
+    for a, x in enumerate(x_refs):
+        produce(a)
+        first.append(
+            send(
+                x.at[pl.ds(theirs, rows)], scratch[a][0], send_sem.at[a * width],
+                recv_sem.at[a * width], "dp", partner,
+            )
+        )
+        if a:
+            cross(a - 1)
+    cross(len(x_refs) - 1)
+    for a in range(len(x_refs)):
         half, own, land, back = scratch[a]
         for copy in second[a]:
             copy.wait()
@@ -117,11 +127,11 @@
             own[pl.ds(r, 16), :] = total.astype(BF16)
         slot = a * width + chips
         third.append(send(own, back, send_sem.at[slot], recv_sem.at[slot], "dp", partner))
-    for a, o in enumerate(o_refs):
+    for a in range(len(x_refs)):
         half, own, land, back = scratch[a]
-        o[pl.ds(mine, rows), :] = own[...]
+        store(a, pl.ds(mine, rows), own[...])
         third[a].wait()
-        o[pl.ds(theirs, rows), :] = back[...]
+        store(a, pl.ds(theirs, rows), back[...])
 
 
 def reduce_scratch(n, shapes):
@@ -138,88 +148,89 @@
     return out + [pltpu.SemaphoreType.DMA((count,)), pltpu.SemaphoreType.DMA((count,))]
 
 
-def dp_kernel(n, main, small, out_main, out_small, *rest):
-    scratch = [rest[0:4], rest[4:8]]
-    reduce_over_dp(n, [main, small], [out_main, out_small], scratch, rest[8:10])
-
-
-def sum_projections(main, small, n, cid):
-    shapes = [main.shape, small.shape]
-    return pl.pallas_call(
-        functools.partial(dp_kernel, n),
-        out_shape=[jax.ShapeDtypeStruct(s, BF16) for s in shapes],
-        in_specs=[VMEM, VMEM],
-        out_specs=[VMEM, VMEM],
-        scratch_shapes=reduce_scratch(n, shapes),
-        compiler_params=params(cid),
-        name="sum_projections",
-    )(main, small)
-
-
-def proj_kernel(where, h, gain, wq, wk, wv, wz, wa, wb, main, small, scaled):
-    @pl.when(pl.program_id(0) == 0)
-    def _():
-        rows = h[...]
-        bent = (rows * gain[...].astype(F32)).astype(BF16)
-        scaled[...] = bent
-        heads = wa.shape[2]
-        both = jnp.concatenate([wa[0], wb[0]], axis=1)
-        small[:, : 2 * heads] = jnp.dot(bent, both, preferred_element_type=F32).astype(BF16)
-        squares = jnp.sum(rows * rows, axis=1, keepdims=True)
-        rest = small.shape[1] - 2 * heads
-        small[:, 2 * heads :] = jnp.broadcast_to(squares, (rows.shape[0], rest)).astype(BF16)
-
-    tile = wq.shape[2]
-    for i, w in enumerate((wq, wk, wv, wz)):
-        main[:, i * tile : (i + 1) * tile] = jnp.dot(
-            scaled[...], w[0], preferred_element_type=F32
-        ).astype(BF16)
-
-
-def project(h, gain, weights, wa, wb, layer, where):
+def proj_kernel(n, layer, h, gain, wab, wq, wk, wv, wz, main, small, wbuf, scaled, w_sem, *rest):
+    feat, cols = wbuf.shape[1:]
+    tile = min(256, cols)
+    chunks = cols // tile
+    loads = []
+    for j in range(chunks):
+        for i, w in enumerate((wq, wk, wv, wz)):
+            at = pl.ds(j * tile, tile)
+            load = pltpu.make_async_copy(w.at[layer, :, at], wbuf.at[i, :, at], w_sem.at[4 * j + i])
+            load.start()
+            loads.append(load)
+    core, partner, others = dp_partners(n)
+    greet("dp", [partner] + others)
+    count = chunks + 1
+    x_refs = rest[:count]
+    scratch = [rest[count + 4 * a : count + 4 * a + 4] for a in range(count)]
+    pair = wab.shape[2]
+
+    def produce(a):
+        x = x_refs[a]
+        if a == 0:
+            rows = h[...]
+            bent = (rows * gain[...].astype(F32)).astype(BF16)
+            scaled[...] = bent
+            x[:, :pair] = jnp.dot(bent, wab[layer], preferred_element_type=F32).astype(BF16)
+            squares = jnp.sum(rows * rows, axis=1, keepdims=True)
+            x[:, pair:] = jnp.broadcast_to(squares, (rows.shape[0], x.shape[1] - pair)).astype(BF16)
+            return
+        j = a - 1
+        for i in range(4):
+            loads[4 * j + i].wait()
+            x[:, i * tile : (i + 1) * tile] = jnp.dot(
+                scaled[...], wbuf[i, :, j * tile : (j + 1) * tile], preferred_element_type=F32
+            ).astype(BF16)
+
+    def store(a, at, val):
+        if a == 0:
+            small[at, :] = val
+        else:
+            main[at, (a - 1) * 4 * tile : a * 4 * tile] = val
+
+    reduce_over_dp(n, produce, x_refs, store, scratch, rest[-2:])
+
+
+def project(h, gain, weights, wab, layer, n, cid):
     rows, feat = h.shape
     cols = weights[0].shape[2]
     tile = min(256, cols)
-    heads = wa.shape[2]
-    wide = pl.BlockSpec((1, feat, tile), lambda j, s: (layer, 0, j))
-    thin = pl.BlockSpec((1, feat, heads), lambda j, s: (layer, s[0], 0))
+    chunks = cols // tile
+    shapes = [(rows, wab.shape[2] + 128)] + [(rows, 4 * tile)] * chunks
     return pl.pallas_call(
-        proj_kernel,
+        functools.partial(proj_kernel, n, layer),
         out_shape=[
             jax.ShapeDtypeStruct((rows, 4 * cols), BF16),
-            jax.ShapeDtypeStruct((rows, 2 * heads + 128), BF16),
+            jax.ShapeDtypeStruct(shapes[0], BF16),
         ],
-        grid_spec=pltpu.PrefetchScalarGridSpec(
-            num_scalar_prefetch=1,
-            grid=(cols // tile,),
-            in_specs=[
-                pl.BlockSpec((rows, feat), lambda j, s: (0, 0)),
-                pl.BlockSpec((1, feat), lambda j, s: (0, 0)),
-                wide, wide, wide, wide, thin, thin,
-            ],
-            out_specs=[
-                pl.BlockSpec((rows, 4 * tile), lambda j, s: (0, j)),
-                pl.BlockSpec((rows, 2 * heads + 128), lambda j, s: (0, 0)),
-            ],
-            scratch_shapes=[pltpu.VMEM((rows, feat), BF16)],
-        ),
+        in_specs=[VMEM, VMEM, VMEM] + [pl.BlockSpec(memory_space=pl.ANY)] * 4,
+        out_specs=[VMEM, VMEM],
+        scratch_shapes=[
+            pltpu.VMEM((4, feat, cols), BF16),
+            pltpu.VMEM((rows, feat), BF16),
+            pltpu.SemaphoreType.DMA((4 * chunks,)),
+            *[pltpu.VMEM(shape, BF16) for shape in shapes],
+            *reduce_scratch(n, shapes),
+        ],
+        compiler_params=params(cid),
         name="project",
-    )(where, h, gain, *weights, wa, wb)
+    )(h, gain, wab, *weights)
 
 
 def recur_kernel(
     width, size, head_size, heads_all, counts, where, main, small, pos_col, pos_row, speed, bias,
     shrink, gain, state, carried, y, new, q_s, k_s, v_s, z_s, dec_s, beta_s, o_s,
 ):
-    seq = pl.program_id(0)
-    slots = q_s.shape[0] // pl.num_programs(0)
+    group = state.shape[1]
+    slots = q_s.shape[0] // (pl.num_programs(0) * group)
     tile = min(256, q_s.shape[1])
     cols = q_s.shape[1]
     row = lax.broadcasted_iota(jnp.int32, (tile, tile), 0) // head_size
     col = lax.broadcasted_iota(jnp.int32, (tile, tile), 1) // head_size
     blocks = (row == col).astype(BF16)
 
-    @pl.when(seq == 0)
+    @pl.when(pl.program_id(0) == 0)
     def _():
         own = q_s.shape[0]
         packed = main.shape[0]
@@ -269,31 +280,32 @@
     key_row = lax.broadcasted_iota(jnp.int32, (size, tile), 0)
     key_col = lax.rem(lax.broadcasted_iota(jnp.int32, (size, tile), 1), head_size)
     diag = key_row == key_col
-    count = counts[seq]
-    for t in range(slots):
-
-        @pl.when(t < count)
-        def _():
-            at = pl.ds(seq * slots + t, 1)
-            for j in range(cols // tile):
-                here = slice(j * tile, (j + 1) * tile)
-                kq = jnp.concatenate(
-                    [
-                        jnp.where(diag, jnp.broadcast_to(k_s[at, here], (size, tile)), 0.0),
-                        jnp.where(diag, jnp.broadcast_to(q_s[at, here], (size, tile)), 0.0),
-                    ],
-                    axis=0,
-                ).astype(BF16)
-                kq = jnp.dot(kq, blocks, preferred_element_type=F32)
-                kmat, qmat = kq[:size], kq[size:]
-                decayed = new[0, 0, :, here] * dec_s[at, here]
-                guess = jnp.sum(decayed * kmat, axis=0, keepdims=True)
-                fresh = beta_s[at, here] * (v_s[at, here] - guess)
-                updated = decayed + kmat * fresh
-                new[0, 0, :, here] = updated
-                o_s[at, here] = jnp.sum(updated * qmat, axis=0, keepdims=True)
-
-    @pl.when(seq == pl.num_programs(0) - 1)
+    for g in range(group):
+        seq = pl.program_id(0) * group + g
+        for t in range(slots):
+
+            @pl.when(t < counts[seq])
+            def _():
+                at = pl.ds(seq * slots + t, 1)
+                for j in range(cols // tile):
+                    here = slice(j * tile, (j + 1) * tile)
+                    kq = jnp.concatenate(
+                        [
+                            jnp.where(diag, jnp.broadcast_to(k_s[at, here], (size, tile)), 0.0),
+                            jnp.where(diag, jnp.broadcast_to(q_s[at, here], (size, tile)), 0.0),
+                        ],
+                        axis=0,
+                    ).astype(BF16)
+                    kq = jnp.dot(kq, blocks, preferred_element_type=F32)
+                    kmat, qmat = kq[:size], kq[size:]
+                    decayed = new[0, g, :, here] * dec_s[at, here]
+                    guess = jnp.sum(decayed * kmat, axis=0, keepdims=True)
+                    fresh = beta_s[at, here] * (v_s[at, here] - guess)
+                    updated = decayed + kmat * fresh
+                    new[0, g, :, here] = updated
+                    o_s[at, here] = jnp.sum(updated * qmat, axis=0, keepdims=True)
+
+    @pl.when(pl.program_id(0) == pl.num_programs(0) - 1)
     def _():
         own = q_s.shape[0]
         packed = main.shape[0]
@@ -308,12 +320,13 @@
 
 def recur(counts, where, main, small, pos, speed, bias, shrink, gain, states, carried, layer, width, heads_all):
     own_seqs = counts.shape[0]
+    group = 2 if own_seqs % 2 == 0 else 1
     packed = main.shape[0]
     size, cols = states.shape[2:]
     own = pos.shape[0]
     heads = speed.shape[1]
     whole = lambda shape: pl.BlockSpec(shape, lambda s, *_: (0,) * len(shape))
-    here = pl.BlockSpec((1, 1, size, cols), lambda s, *_: (layer, s, 0, 0))
+    here = pl.BlockSpec((1, group, size, cols), lambda s, *_: (layer, s, 0, 0))
     args = [main, small, pos[:, None], pos[None, :], speed, bias, shrink, gain]
     specs = [whole(a.shape) for a in args] + [here]
     kernel = functools.partial(recur_kernel, width, size, cols // heads, heads_all)
@@ -332,7 +345,7 @@
         ],
         grid_spec=pltpu.PrefetchScalarGridSpec(
             num_scalar_prefetch=2,
-            grid=(own_seqs,),
+            grid=(own_seqs // group,),
             in_specs=specs,
             out_specs=[whole((packed, cols)), here],
             scratch_shapes=[pltpu.VMEM((own, cols), F32) for _ in range(7)],
@@ -342,28 +355,28 @@
     )(counts, where, *args, states, *more)
 
 
-def gated_kernel(n, y, out, *rest):
-    reduce_over_dp(n, [y], [out], [rest[0:4]], rest[4:6])
-
-
-def share_gated(y, n, cid):
-    return pl.pallas_call(
-        functools.partial(gated_kernel, n),
-        out_shape=jax.ShapeDtypeStruct(y.shape, BF16),
-        in_specs=[VMEM],
-        out_specs=VMEM,
-        scratch_shapes=reduce_scratch(n, [y.shape]),
-        compiler_params=params(cid),
-        name="share_gated",
-    )(y)
-
-
-def mix_kernel(m, gated, w, h, out, part, land, own, gath, send_a, recv_a, send_b, recv_b):
+def mix_kernel(
+    n, m, layer, y, w, h, out, wbuf, w_sem, gated, part, land, own, gath,
+    send_a, recv_a, send_b, recv_b, *rest,
+):
+    load = pltpu.make_async_copy(w.at[layer], wbuf, w_sem)
+    load.start()
     me = lax.axis_index("tp")
     peers = [lax.rem(me + d, m) for d in range(1, m)]
-    greet("tp", peers)
+    core, partner, others = dp_partners(n)
+    barrier = pltpu.get_barrier_semaphore()
+    for axis, group in (("dp", [partner] + others), ("tp", peers)):
+        for peer in group:
+            pl.semaphore_signal(barrier, inc=1, device_id={axis: peer}, device_id_type=MESH)
+    pl.semaphore_wait(barrier, 1 + len(others) + len(peers))
+
+    def store(a, at, val):
+        gated[at, :] = val
+
+    reduce_over_dp(n, lambda a: None, [y], store, [rest[0:4]], rest[4:6])
+    load.wait()
     rows = part.shape[1]
-    mixed = jnp.dot(gated[...], w[0], preferred_element_type=F32)
+    mixed = jnp.dot(gated[...], wbuf[...], preferred_element_type=F32)
     for j in range(m):
         part[j] = mixed[j * rows : (j + 1) * rows].astype(BF16)
     copies = [
@@ -387,31 +400,28 @@
         out[at, :] = (h[at, :] + gath[j].astype(F32)).astype(BF16).astype(F32)
 
 
-def mix(gated, w, h, layer, m, cid):
+def mix(y, w, h, layer, n, m, cid):
     packed, feat = h.shape
-    cols = gated.shape[1]
     rows = packed // m
-    once = lambda shape: pl.BlockSpec(shape, lambda i: (0,) * len(shape))
     return pl.pallas_call(
-        functools.partial(mix_kernel, m),
-        grid=(1,),
+        functools.partial(mix_kernel, n, m, layer),
         out_shape=jax.ShapeDtypeStruct(h.shape, F32),
-        in_specs=[
-            once(gated.shape),
-            pl.BlockSpec((1, cols, feat), lambda i: (layer, 0, 0)),
-            once(h.shape),
-        ],
-        out_specs=once(h.shape),
+        in_specs=[VMEM, pl.BlockSpec(memory_space=pl.ANY), VMEM],
+        out_specs=VMEM,
         scratch_shapes=[
+            pltpu.VMEM(w.shape[1:], BF16),
+            pltpu.SemaphoreType.DMA,
+            pltpu.VMEM(y.shape, BF16),
             pltpu.VMEM((m, rows, feat), BF16),
             pltpu.VMEM((m - 1, rows, feat), BF16),
             pltpu.VMEM((rows, feat), BF16),
             pltpu.VMEM((m, rows, feat), BF16),
             *[pltpu.SemaphoreType.DMA((m - 1,)) for _ in range(4)],
+            *reduce_scratch(n, [y.shape]),
         ],
         compiler_params=params(cid),
         name="mix",
-    )(gated, w, h)
+    )(y, w, h)
 
 
 def body(
@@ -446,6 +456,8 @@
     dp = lax.axis_index("dp")
     where = jnp.stack([dp, lax.axis_index("tp")]).astype(jnp.int32)
     every = gather_counts(counts, n, 1)
+    cut = lambda w: lax.dynamic_slice_in_dim(w, dp * feat, feat, 1)
+    wab = jnp.concatenate([cut(wa), cut(wb)], axis=2)
     before = lax.broadcasted_iota(jnp.int32, (all_seqs, all_seqs), 1) < lax.broadcasted_iota(
         jnp.int32, (all_seqs, all_seqs), 0
     )
@@ -458,15 +470,13 @@
     h = jnp.dot(onehot, flat, preferred_element_type=F32)
     carried = None
     for l in range(BLOCKS):
-        main, small = project(h, scaling[l][None], (wq, wk, wv, wz), wa, wb, l, where)
-        main, small = sum_projections(main, small, n, 2 + 3 * l)
+        main, small = project(h, scaling[l][None], (wq, wk, wv, wz), wab, l, n, 2 + 2 * l)
         gain = jnp.tile(channel[l].astype(F32), heads)[None]
         y, carried = recur(
             counts, where, main, small, pos_own, speed[l][None], bias[l][None],
             shrink[l].reshape(own, heads), gain, states, carried, l, feat * n, wa.shape[2],
         )
-        gated = share_gated(y, n, 3 + 3 * l)
-        h = mix(gated, wo, h, l, m, 4 + 3 * l)
+        h = mix(y, wo, h, l, n, m, 3 + 2 * l)
     back = lax.dot_general(
         onehot, h.astype(BF16), (((0,), (0,)), ((), ())), preferred_element_type=F32
     )

time: 159 us -> 130 us (0.82)
  Pallas kernels: 129 us -> 107 us
  local copies, waits for them, and re-layouts: 25.9 us -> 18.6 us
    pallas_call x8 -> x4, Pallas kernels: 88.9 us -> 76.1 us  [the longest x2 44.4 us: mix(): pl.pallas_call(functools.partial(mix_kernel, n, m, layer), out_shape=jax....]
    pallas_call x2, Pallas kernels: 35.5 us -> 26.6 us  [recur(): pl.pallas_call(body, out_shape=[jax.ShapeDtypeStruct((packed, cols), BF16...]
    unnamed x44 -> x36, local copies, waits for them, and re-layouts: 18.3 us -> 12.3 us
where the time goes in v2:
time: 130 us; the launch traced here: 129 us
  Pallas kernels  107 us (82%)
  local copies, waits for them, and re-layouts  18.6 us (14%)
    pallas_call x2, Pallas kernels, mix(): pl.pallas_call(functools.partial(mix_kernel, n, m, layer), out_shape=jax....  44.4 us
    pallas_call x2, Pallas kernels, project(): pl.pallas_call(functools.partial(proj_kernel, n, layer), out_shape=[jax.S...  31.7 us
    pallas_call x2, Pallas kernels, recur(): pl.pallas_call(body, out_shape=[jax.ShapeDtypeStruct((packed, cols), BF16...  26.6 us
    unnamed x36, local copies, waits for them, and re-layouts  12.3 us
    pallas_call x1, Pallas kernels, gather_counts(): pl.pallas_call(functools.partial(gather_kernel, n), out_shape=jax.ShapeDt...  4.68 us

profile of v2, /device:TPU:0, one launch (start us, length us, event | category | flops | bytes accessed | tf_op | source)
XLA Modules:
  0.0 128.5 jit_solution(3065554608145373025)
XLA Ops:
  0.6 0.0 copy-start.13
  0.6 0.0 copy-start.10
  0.7 0.0 copy-start.12
  0.7 1.1 constant_dynamic-slice_fusion
  1.8 0.3 copy.30
  2.1 0.3 copy.31
  2.4 0.3 pad_maximum_fusion.wab
  2.7 0.0 copy-done.13
  2.7 4.7 %gather_counts.1 = s32[4,8,128]{2,1,0:T(8,128)S(1)} custom-call(s32[8,128]{1,0:T(8,128)S(1)} %broadcast_in_dim.39.x_ref), custom_call_target="tpu_custom_call" | custom-call | tf_op jit(solution)/shard_map/gather_counts/pallas_call | solution.py:61
  7.4 0.1 lt.31
  7.5 0.1 select_reduce_fusion
  7.6 0.1 add_select_fusion
  7.7 0.1 select_n.34
  7.8 0.0 copy-done.10
  7.8 0.1 reshape.76
  7.9 0.2 fusion.2.h
  8.2 0.0 copy-done.12
  8.2 0.0 copy-start
  8.2 2.2 %copy-done = bf16[2,1024,1024]{2,1,0:T(8,128)(2,1)S(1)} copy-done((bf16[2,1024,1024]{2,1,0:T(8,128)(2,1)S(1)}, bf16[2,1024,1024]{2,1,0:T(8,128)(2,1)}, u32[]{:S(2)}) %copy-start) | copy-done | bytes 4194328
  10.4 0.0 copy-start.15
  10.4 0.0 copy-start.16
  10.4 0.0 copy-start.11
  10.4 0.0 copy-start.14
  10.4 16.0 %project.2 = (bf16[96,4096]{1,0:T(8,128)(2,1)S(1)}, bf16[96,256]{1,0:T(8,128)(2,1)S(1)}) custom-call(f32[96,1024]{1,0:T(8,128)S(1)} %fusion.2.h, bf16[1,1024]{1,0:T(2,128)(2,1)S(1)} %get-tuple-element.21.gain, bf16[2,1024,128]{2,1,0:T(8,128)(2,1)S(1)} %pad_maximum_fusion.wab, bf16[2,1024,1024]{2,1,0:T(8,128)(2,1)S(1)} %copy-done, bf16[2,1024,1024]{2,1,0:T(8,128)(2,1)} %wk.3, ...), custom_call_target="tpu_custom_call" | custom-call | tf_op jit(solution)/shard_map/project/pallas_call | solution.py:201
  26.4 0.0 copy-start.4
  26.4 0.9 copy-done.4
  27.3 0.0 copy-start.8
  27.3 0.6 copy-done.8
  27.9 0.6 dynamic-slice_bitcast_fusion
  28.5 0.7 copy.28.refs_4_.pos_col
  29.2 0.6 pad_add_fusion.refs_1_.where
  29.8 0.0 copy-done.15
  29.8 0.0 copy-done.16
  29.8 0.6 fusion.7
  30.4 0.0 copy-done.11
  30.4 0.6 fusion.5
  31.0 0.0 copy-done.14
  31.0 0.7 broadcast_in_dim_tile.6.refs_9_
  31.7 13.2 %recur.2 = (bf16[96,1024]{1,0:T(8,128)(2,1)}, f32[2,16,64,1024]{3,2,1,0:T(8,128)}) custom-call(s32[16]{0:T(128)} %counts.1, s32[2]{0:T(128)} %pad_add_fusion.refs_1_.where, bf16[96,4096]{1,0:T(8,128)(2,1)} %copy-done.4, bf16[96,256]{1,0:T(8,128)(2,1)} %copy-done.8, s32[64,1]{1,0:T(8,128)} %copy.28.refs_4_.pos_col, ...), custom_call_target="tpu_custom_call" | custom-call | tf_op jit(solution)/shard_map/recur/pallas_call | solution.py:340
  44.9 0.0 copy-start.1
  44.9 0.0 copy-start.2
  44.9 2.3 %copy-done.2 = bf16[2,1024,1024]{2,1,0:T(8,128)(2,1)S(1)} copy-done((bf16[2,1024,1024]{2,1,0:T(8,128)(2,1)S(1)}, bf16[2,1024,1024]{2,1,0:T(8,128)(2,1)}, u32[]{:S(2)}) %copy-start.2) | copy-done | bytes 4194328
  47.3 0.0 copy-start.7
  47.3 1.1 copy-done.7
  48.4 23.2 %mix.2.h = f32[96,1024]{1,0:T(8,128)S(1)} custom-call(bf16[96,1024]{1,0:T(8,128)(2,1)S(1)} %copy-done.7, bf16[2,1024,1024]{2,1,0:T(8,128)(2,1)S(1)} %copy-done.2, f32[96,1024]{1,0:T(8,128)S(1)} %fusion.2.h), custom_call_target="tpu_custom_call" | custom-call | tf_op jit(solution)/shard_map/mix/pallas_call | solution.py:406
  71.6 0.0 copy-done.1
  71.6 15.7 %project.3 = (bf16[96,4096]{1,0:T(8,128)(2,1)S(1)}, bf16[96,256]{1,0:T(8,128)(2,1)S(1)}) custom-call(f32[96,1024]{1,0:T(8,128)S(1)} %mix.2.h, bf16[1,1024]{1,0:T(2,128)(2,1)S(1)} %get-tuple-element.20.gain, bf16[2,1024,128]{2,1,0:T(8,128)(2,1)S(1)} %pad_maximum_fusion.wab, bf16[2,1024,1024]{2,1,0:T(8,128)(2,1)S(1)} %copy-done.1, bf16[2,1024,1024]{2,1,0:T(8,128)(2,1)} %wk.3, ...), custom_call_target="tpu_custom_call" | custom-call | tf_op jit(solution)/shard_map/project/pallas_call | solution.py:201
  87.3 0.0 copy-start.5
  87.3 0.9 copy-done.5
  88.2 0.0 copy-start.9
  88.2 0.6 copy-done.9
  88.8 0.7 broadcast_in_dim_tile.7.gain
  89.4 13.4 %recur.3 = (bf16[96,1024]{1,0:T(8,128)(2,1)}, f32[2,16,64,1024]{3,2,1,0:T(8,128)}) custom-call(s32[16]{0:T(128)} %counts.1, s32[2]{0:T(128)} %pad_add_fusion.refs_1_.where, bf16[96,4096]{1,0:T(8,128)(2,1)} %copy-done.5, bf16[96,256]{1,0:T(8,128)(2,1)} %copy-done.9, s32[64,1]{1,0:T(8,128)} %copy.28.refs_4_.pos_col, ...), custom_call_target="tpu_custom_call", output_to_operand_aliasing={{1}: (11, {})} | custom-call | tf_op jit(solution)/shard_map/recur/pallas_call | solution.py:340
  102.8 0.0 copy-start.3
  102.8 2.2 %copy-done.3 = bf16[2,1024,1024]{2,1,0:T(8,128)(2,1)S(1)} copy-done((bf16[2,1024,1024]{2,1,0:T(8,128)(2,1)S(1)}, bf16[2,1024,1024]{2,1,0:T(8,128)(2,1)}, u32[]{:S(2)}) %copy-start.3) | copy-done | bytes 4194328
  105.0 0.0 copy-start.6
  105.0 0.9 copy-done.6
  106.0 21.2 %mix.3 = f32[96,1024]{1,0:T(8,128)S(1)} custom-call(bf16[96,1024]{1,0:T(8,128)(2,1)S(1)} %copy-done.6, bf16[2,1024,1024]{2,1,0:T(8,128)(2,1)S(1)} %copy-done.3, f32[96,1024]{1,0:T(8,128)S(1)} %mix.2.h), custom_call_target="tpu_custom_call" | custom-call | tf_op jit(solution)/shard_map/mix/pallas_call | solution.py:406
  127.2 0.3 fusion
  127.5 1.0 reshape.77
  (8 shorter events, 0.1 us)
Async XLA Ops:
  0.6 2.0 %copy-start.13 = (s32[16]{0:T(128)S(1)}, s32[16]{0:T(128)}, u32[]{:S(2)}) copy-start(s32[16]{0:T(128)} %counts.1) | copy-start | bytes 196
  0.6 7.2 %copy-start.10 = (bf16[64,4,1024]{2,1,0:T(4,128)(2,1)S(1)}, bf16[64,4,1024]{2,1,0:T(4,128)(2,1)}, u32[]{:S(2)}) copy-start(bf16[64,4,1024]{2,1,0:T(4,128)(2,1)} %param.15) | copy-start | bytes 1572868
  0.7 7.5 %copy-start.12 = (bf16[2,1024]{1,0:T(2,128)(2,1)S(1)}, bf16[2,1024]{1,0:T(2,128)(2,1)}, u32[]{:S(2)}) copy-start(bf16[2,1024]{1,0:T(2,128)(2,1)} %param.26) | copy-start | bytes 12292
  8.2 2.2 %copy-start = (bf16[2,1024,1024]{2,1,0:T(8,128)(2,1)S(1)}, bf16[2,1024,1024]{2,1,0:T(8,128)(2,1)}, u32[]{:S(2)}) copy-start(bf16[2,1024,1024]{2,1,0:T(8,128)(2,1)} %wq.3) | copy-start | bytes 12582916
  10.4 19.4 %copy-start.15 = (f32[2,16]{1,0:T(2,128)S(1)}, f32[2,16]{1,0:T(2,128)}, u32[]{:S(2)}) copy-start(f32[2,16]{1,0:T(2,128)} %param.25) | copy-start | bytes 388
  10.4 19.4 %copy-start.16 = (f32[2,16]{1,0:T(2,128)S(1)}, f32[2,16]{1,0:T(2,128)}, u32[]{:S(2)}) copy-start(f32[2,16]{1,0:T(2,128)} %param.24) | copy-start | bytes 388
  10.4 20.0 %copy-start.11 = (f32[2,16,4,16]{3,2,1,0:T(4,128)S(1)}, f32[2,16,4,16]{3,2,1,0:T(4,128)}, u32[]{:S(2)}) copy-start(f32[2,16,4,16]{3,2,1,0:T(4,128)} %param.28) | copy-start | bytes 24580
  10.4 20.7 %copy-start.14 = (bf16[2,64]{1,0:T(2,128)(2,1)S(1)}, bf16[2,64]{1,0:T(2,128)(2,1)}, u32[]{:S(2)}) copy-start(bf16[2,64]{1,0:T(2,128)(2,1)} %param.27) | copy-start | bytes 772
  26.4 0.9 copy-start.4
  27.3 0.6 copy-start.8
  44.9 26.6 %copy-start.1 = (bf16[2,1024,1024]{2,1,0:T(8,128)(2,1)S(1)}, bf16[2,1024,1024]{2,1,0:T(8,128)(2,1)}, u32[]{:S(2)}) copy-start(bf16[2,1024,1024]{2,1,0:T(8,128)(2,1)} %wq.3) | copy-start | bytes 12582916
  44.9 2.3 %copy-start.2 = (bf16[2,1024,1024]{2,1,0:T(8,128)(2,1)S(1)}, bf16[2,1024,1024]{2,1,0:T(8,128)(2,1)}, u32[]{:S(2)}) copy-start(bf16[2,1024,1024]{2,1,0:T(8,128)(2,1)} %w.3) | copy-start | bytes 12582916
  47.3 1.1 copy-start.7
  87.3 0.9 copy-start.5
  88.2 0.6 copy-start.9
  102.8 2.2 %copy-start.3 = (bf16[2,1024,1024]{2,1,0:T(8,128)(2,1)S(1)}, bf16[2,1024,1024]{2,1,0:T(8,128)(2,1)}, u32[]{:S(2)}) copy-start(bf16[2,1024,1024]{2,1,0:T(8,128)(2,1)} %w.3) | copy-start | bytes 12582916
  105.0 0.9 copy-start.6
